TPU v7x, 32 devices: a whole 2x2x4 slice. The times are simulated.
32 devices in a mesh: sp: 8 (over z, core), tp: 4 (over y, x).
Axes of the slice: x: 2, y: 2, z: 4, core: 2. Of those that a mesh axis runs over, the one named last changes fastest.
Arguments:
- cotangent: bfloat16 [1024, 2048], P('sp'), may hold values from -6 to 6
- normed: bfloat16 [1024, 2048], P('sp'), may hold values from -6 to 6
- inverse_root_mean_square: float32 [1024], P('sp'), may hold values from 0.5 to 2
- expert_norm_scale: float32 [2048], replicated, may hold values from 0.1 to 1.9
- routes: int32 [1024, 2], P('sp'), may hold values from 0 to 7, all different within a row; in each aligned block of 128 rows (0 to 127, 128 to 255, ...) at most 64 rows name the same one
- route_probability_weight: float32 [1024, 2], P('sp'), may hold values from 0.2 to 1
- gate_weight: bfloat16 [8, 2048, 2048], P('sp', None, 'tp'), may hold values from -0.125 to 0.125
- up_weight: bfloat16 [8, 2048, 2048], P('sp', None, 'tp'), may hold values from -0.125 to 0.125
- down_weight: bfloat16 [8, 2048, 2048], P('sp', 'tp'), may hold values from -0.125 to 0.125
- recurrence_input: bfloat16 [1024, 1024], P('sp', 'tp'), may hold values from -6 to 6
- recurrence_gate_logits: bfloat16 [1024, 1024], P('sp', 'tp'), may hold values from -6 to 6
- input_gate_logits: bfloat16 [1024, 1024], P('sp', 'tp'), may hold values from -6 to 6
- channel_decay_weight: float32 [1024], P('tp'), may hold values from 3 to 20
- extra_log_decay: float32 [1024, 1024], P('sp', 'tp'), may hold values from -1 to 0
- output_matrix: bfloat16 [2048, 1024], P(None, 'tp'), may hold values from -0.1875 to 0.1875
Outputs:
- grad_gate: bfloat16 [8, 2048, 2048], P('sp', None, 'tp')
- grad_up: bfloat16 [8, 2048, 2048], P('sp', None, 'tp')
- grad_down: bfloat16 [8, 2048, 2048], P('sp', 'tp')
- grad_out_weight: float32 [2048, 1024], P('sp', 'tp')
- grad_rec_input: float32 [1024, 1024], P('sp', 'tp')
- grad_decay_gate: float32 [1024, 1024], P('sp', 'tp')
- grad_input_gate: float32 [1024, 1024], P('sp', 'tp')
Inputs may be any that keep to these rules, and one draw needn't show every extreme that they name: `routes`: each row names 2 different experts; among the rows of one device no expert is named more than 64 times.
All inputs are finite; a program needn't handle non-finite values.
Results may differ from a plain program's by a relative error of at most 0.025.
Values may be sent and summed in bfloat16 or wider, within the bound.
A program may use at most 64 MiB of HBM per device.

v0:
```python
import jax
import jax.numpy as jnp
from jax import lax
from jax.sharding import PartitionSpec as P


def carried_in(part, axis, combine, identity, reverse):
    count = lax.axis_size(axis)
    place = lax.axis_index(axis)
    ahead = count - 1 - place if reverse else place
    gathered = jax.tree.map(lambda a: lax.all_gather(a, axis), part)
    state = jax.tree.map(lambda a, e: jnp.zeros_like(a) + jnp.asarray(e, a.dtype), part, identity)

    def one(turn, state):
        source = count - 1 - turn if reverse else turn
        return combine(
            state, jax.tree.map(lambda a: lax.dynamic_index_in_dim(a, source, 0, False), gathered)
        )

    return lax.fori_loop(0, ahead, one, state)


def link(earlier, later):
    return (earlier[0] * later[0], later[0] * earlier[1] + later[1])


def shards(
    cotangent,
    normed,
    inverse_root_mean_square,
    expert_norm_scale,
    routes,
    route_probability_weight,
    gate_weight,
    up_weight,
    down_weight,
    recurrence_input,
    recurrence_gate_logits,
    input_gate_logits,
    channel_decay_weight,
    extra_log_decay,
    output_matrix,
):
    tok_rows, features = normed.shape
    groups = lax.axis_size("sp")
    picks = routes.shape[1]
    capacity = 2 * picks * tok_rows // groups
    rowdims = (((0,), (0,)), ((), ()))
    coldims = (((1,), (1,)), ((), ()))
    chosen = routes.reshape(-1)
    member = (chosen[:, None] == jnp.arange(groups, dtype=jnp.int32)[None, :]).astype(jnp.int32)
    ranking = jnp.sum((jnp.cumsum(member, axis=0) - member) * member, axis=1)
    landing = chosen * capacity + ranking
    scaled = (
        route_probability_weight[:, :, None] * cotangent[:, None, :].astype(jnp.float32)
    ).astype(jnp.bfloat16)
    scaled = scaled.reshape(tok_rows * picks, features)
    copies = jnp.repeat(normed, picks, axis=0)
    grad_send = jnp.zeros((groups * capacity, features), jnp.bfloat16).at[landing].set(scaled)
    token_send = jnp.zeros((groups * capacity, features), jnp.bfloat16).at[landing].set(copies)
    grad_recv, token_recv = (
        lax.all_to_all(grad_send, "sp", split_axis=0, concat_axis=0, tiled=True),
        lax.all_to_all(token_send, "sp", split_axis=0, concat_axis=0, tiled=True),
    )
    gate_w = gate_weight[0]
    up_w = up_weight[0]
    down_w = down_weight[0]
    gate_pre = jnp.dot(token_recv, gate_w, preferred_element_type=jnp.float32)
    up_pre = jnp.dot(token_recv, up_w, preferred_element_type=jnp.float32)
    sigma = jax.nn.sigmoid(gate_pre)
    swish = gate_pre * sigma
    active = (swish * up_pre).astype(jnp.bfloat16)
    d_active = lax.dot_general(grad_recv, down_w, coldims, preferred_element_type=jnp.float32)
    d_gate = (d_active * up_pre * sigma * (1.0 + gate_pre * (1.0 - sigma))).astype(jnp.bfloat16)
    d_up = (d_active * swish).astype(jnp.bfloat16)
    grad_down = lax.dot_general(
        active, grad_recv, rowdims, preferred_element_type=jnp.float32
    ).astype(jnp.bfloat16)
    grad_gate = lax.dot_general(
        token_recv, d_gate, rowdims, preferred_element_type=jnp.float32
    ).astype(jnp.bfloat16)
    grad_up = lax.dot_general(token_recv, d_up, rowdims, preferred_element_type=jnp.float32).astype(
        jnp.bfloat16
    )
    partial_rows = lax.dot_general(d_gate, gate_w, coldims, preferred_element_type=jnp.float32)
    partial_rows = partial_rows + lax.dot_general(
        d_up, up_w, coldims, preferred_element_type=jnp.float32
    )
    shared = lax.psum_scatter(
        partial_rows.astype(jnp.bfloat16), "tp", scatter_dimension=1, tiled=True
    )
    returned = lax.all_to_all(shared, "sp", split_axis=0, concat_axis=0, tiled=True)
    slice_width = returned.shape[1]
    offset = lax.axis_index("tp") * slice_width
    gain_part = lax.dynamic_slice_in_dim(expert_norm_scale, offset, slice_width, 0)
    normed_part = lax.dynamic_slice_in_dim(normed, offset, slice_width, 1)
    cot_part = lax.dynamic_slice_in_dim(cotangent, offset, slice_width, 1)
    d_norm = jnp.sum(
        returned[landing].astype(jnp.float32).reshape(tok_rows, picks, slice_width), axis=1
    )
    nhat = normed_part.astype(jnp.float32) / gain_part[None, :]
    gained = gain_part[None, :] * d_norm
    stat = lax.psum(jnp.sum(gained * nhat, axis=1), "tp")[:, None] / features
    mix_part = (
        cot_part.astype(jnp.float32) + inverse_root_mean_square[:, None] * (gained - nhat * stat)
    ).astype(jnp.bfloat16)
    d_mix = lax.all_gather(mix_part, "tp", axis=1, tiled=True)
    retention_factor = jax.nn.sigmoid(recurrence_gate_logits.astype(jnp.float32))
    admit = jax.nn.sigmoid(input_gate_logits.astype(jnp.float32))
    signal = recurrence_input.astype(jnp.float32)
    decay_speed = jax.nn.softplus(-channel_decay_weight)
    log_retention = -8.0 * retention_factor * decay_speed[None, :] + extra_log_decay
    keep = jnp.exp(log_retention)
    scale_in = jnp.sqrt(-jnp.expm1(2.0 * log_retention))
    driven = scale_in * admit * signal
    channels = keep.shape[1]
    identity = (jnp.ones((channels,), jnp.float32), jnp.zeros((channels,), jnp.float32))
    keep_cum, state_loc = lax.associative_scan(link, (keep, driven), axis=0)
    _, state_in = carried_in((keep_cum[-1], state_loc[-1]), "sp", link, identity, False)
    state = state_loc + keep_cum * state_in[None, :]
    hidden = state.astype(jnp.bfloat16)
    state_prev = jnp.concatenate([state_in[None, :], state[:-1]], axis=0)
    grad_out_weight = lax.psum_scatter(
        lax.dot_general(d_mix, hidden, rowdims, preferred_element_type=jnp.float32).astype(
            jnp.bfloat16
        ),
        "sp",
        scatter_dimension=0,
        tiled=True,
    ).astype(jnp.float32)
    d_state = jnp.dot(d_mix, output_matrix, preferred_element_type=jnp.float32)
    keep_next = jnp.concatenate([keep[1:], jnp.ones((1, channels), jnp.float32)], axis=0)
    tail_keep, grad_loc = lax.associative_scan(link, (keep_next, d_state), reverse=True, axis=0)
    block_map = (keep[0] * tail_keep[0], keep[0] * grad_loc[0])
    _, grad_enter = carried_in(block_map, "sp", link, identity, True)
    total = grad_loc + tail_keep * grad_enter[None, :]
    grad_rec_input = total * scale_in * admit
    grad_input_gate = total * scale_in * signal * admit * (1.0 - admit)
    d_log = total * state_prev * keep - total * admit * signal * keep * keep / scale_in
    grad_decay_gate = (
        d_log * (-8.0 * decay_speed[None, :]) * retention_factor * (1.0 - retention_factor)
    )
    return (
        grad_gate[None],
        grad_up[None],
        grad_down[None],
        grad_out_weight,
        grad_rec_input,
        grad_decay_gate,
        grad_input_gate,
    )


def solution(mesh):
    return jax.shard_map(
        shards,
        mesh=mesh,
        in_specs=(
            P("sp", None),
            P("sp", None),
            P("sp"),
            P(),
            P("sp", None),
            P("sp", None),
            P("sp", None, "tp"),
            P("sp", None, "tp"),
            P("sp", "tp", None),
            P("sp", "tp"),
            P("sp", "tp"),
            P("sp", "tp"),
            P("tp"),
            P("sp", "tp"),
            P(None, "tp"),
        ),
        out_specs=(
            P("sp", None, "tp"),
            P("sp", None, "tp"),
            P("sp", "tp", None),
            P("sp", "tp"),
            P("sp", "tp"),
            P("sp", "tp"),
            P("sp", "tp"),
        ),
        check_vma=False,
    )
```

profile of v0, /device:TPU:0, one launch (start us, length us, event | category | flops | bytes accessed | tf_op | source)
XLA Modules:
  0.0 311.9 jit_solution(7391208926306935879)
XLA Ops:
  10.2 1.7 broadcast_in_dim.10
  11.9 1.2 reshape.104
  13.2 4.4 %scatter_custom_fusion = bf16[512,2048]{1,0:T(8,128)(2,1)} fusion(s32[256]{0:T(256)S(1)} %bitcast.98, bf16[256,2048]{1,0:T(8,128)(2,1)} %reshape.104, bf16[]{:T(256)} %constant.74.clone.1), kind=kCustom, calls=%fused_computation.35 | custom fusion | bytes 2097664 | tf_op jit(solution)/shard_map/scatter | solution.py:60
  17.6 6.5 %all-to-all-start = ((bf16[8,64,2048]{2,1,0:T(8,128)(2,1)}), bf16[8,64,2048]{2,1,0:T(8,128)(2,1)}, u32[]{:S(2)}, u32[]{:S(2)}) async-start(bf16[8,64,2048]{2,1,0:T(8,128)(2,1)} %bitcast.86), calls=%async_computation | async-start | bytes 4194304 | tf_op jit(solution)/shard_map/all_to_all | solution.py:63
  24.1 2.4 mul.362
  26.5 3.7 %mul.363 = f32[256,2048]{1,0:T(8,128)} reshape(f32[128,2,2048]{2,1,0:T(2,128)} %mul.362) | data formatting | bytes 4194304 | tf_op jit(solution)/shard_map/mul | solution.py:55
  30.4 4.8 %scatter_custom_fusion.1 = bf16[512,2048]{1,0:T(8,128)(2,1)} fusion(s32[256]{0:T(256)S(1)} %bitcast.99, f32[256,2048]{1,0:T(8,128)} %mul.363, f32[256]{0:T(256)S(1)} %mul.360, bf16[]{:T(256)} %constant.74.clone.1), kind=kCustom, calls=%fused_computation.27 | custom fusion | flops 1048576 | bytes 4195330 | tf_op jit(solution)/shard_map/scatter | solution.py:59
  35.2 38.0 %all-to-all-done = bf16[8,64,2048]{2,1,0:T(8,128)(2,1)} async-done(((bf16[8,64,2048]{2,1,0:T(8,128)(2,1)}), bf16[8,64,2048]{2,1,0:T(8,128)(2,1)}, u32[]{:S(2)}, u32[]{:S(2)}) %all-to-all-start) | async-done | bytes 2097184 | tf_op jit(solution)/shard_map/all_to_all | solution.py:63
  73.2 4.5 %all-to-all-start.1 = ((bf16[8,64,2048]{2,1,0:T(8,128)(2,1)}), bf16[8,64,2048]{2,1,0:T(8,128)(2,1)}, u32[]{:S(2)}, u32[]{:S(2)}) async-start(bf16[8,64,2048]{2,1,0:T(8,128)(2,1)} %bitcast.85), calls=%async_computation.1 | async-start | bytes 4194304 | tf_op jit(solution)/shard_map/all_to_all | solution.py:62
  80.9 4.0 %fusion.5 = f32[512,512]{1,0:T(8,128)} fusion(bf16[512,2048]{1,0:T(8,128)(2,1)} %bitcast.9, bf16[1,2048,512]{2,1,0:T(8,128)(2,1)S(1)} %copy-done), kind=kOutput, calls=%fused_computation.19 | convolution fusion | flops 1073741824 | bytes 5242880 | tf_op jit(solution)/shard_map/dot_general | solution.py:68
  84.9 3.8 %fusion.8 = f32[512,512]{1,0:T(8,128)} fusion(bf16[512,2048]{1,0:T(8,128)(2,1)} %bitcast.9, bf16[1,2048,512]{2,1,0:T(8,128)(2,1)S(1)} %copy-done.1), kind=kOutput, calls=%fused_computation.22 | convolution fusion | flops 1073741824 | bytes 5242880 | tf_op jit(solution)/shard_map/dot_general | solution.py:69
  88.7 38.1 %all-to-all-done.1 = bf16[8,64,2048]{2,1,0:T(8,128)(2,1)} async-done(((bf16[8,64,2048]{2,1,0:T(8,128)(2,1)}), bf16[8,64,2048]{2,1,0:T(8,128)(2,1)}, u32[]{:S(2)}, u32[]{:S(2)}) %all-to-all-start.1) | async-done | bytes 2097184 | tf_op jit(solution)/shard_map/all_to_all | solution.py:62
  126.8 4.4 %multiply_convert_fusion.3 = (bf16[512,512]{1,0:T(8,128)(2,1)S(1)}, bf16[512,512]{1,0:T(8,128)(2,1)S(1)}) fusion(f32[512,512]{1,0:T(8,128)} %fusion.5, f32[512,512]{1,0:T(8,128)} %fusion.8, bf16[512,2048]{1,0:T(8,128)(2,1)} %bitcast.11, bf16[1,512,2048]{2,1,0:T(8,128)(2,1)} %param.27), kind=kOutput, calls=%fused_computation.29 | convolution fusion | flops 1077149696 | bytes 7340032 | tf_op jit(solution)/shard_map/dot_general | solution.py:73
  131.2 1.3 fusion.3
  132.9 2.6 add_convert_fusion
  138.6 1.3 pad.187
  139.9 29.9 %reduce-scatter.3.cloned.1.call-done = bf16[512,512]{1,0:T(8,128)(2,1)} async-done(((bf16[512,2048]{1,0:T(8,128)(2,1)}), bf16[512,512]{1,0:T(8,128)(2,1)}) %reduce-scatter.3.cloned.1.call-update) | async-done | bytes 524304 | tf_op jit(solution)/shard_map/reduce_scatter | solution.py:89
  169.8 4.6 %all-to-all-start.2 = ((bf16[8,64,512]{2,1,0:T(8,128)(2,1)}), bf16[8,64,512]{2,1,0:T(8,128)(2,1)S(1)}, u32[]{:S(2)}, u32[]{:S(2)}) async-start(bf16[8,64,512]{2,1,0:T(8,128)(2,1)} %bitcast.88), calls=%async_computation.3 | async-start | bytes 1048576 | tf_op jit(solution)/shard_map/all_to_all | solution.py:92
  178.0 1.4 slice.526
  179.4 1.4 slice.519
  180.8 1.4 slice.517
  182.2 12.2 %all-gather.1 = f32[8,1,256]{2,1,0:T(1,128)S(1)} all-gather(f32[1,1,256]{2,1,0:T(1,128)S(1)} %add_bitcast_fusion), channel_id=1, replica_groups=mesh['sp'=8,'tp'=4] {'sp'}, dimensions={0}, use_global_device_ids=true | all-gather | bytes 9216 | tf_op jit(solution)/shard_map/all_gather | solution.py:11
  195.7 1.3 pad.201
  197.1 4.3 %fusion = bf16[1,2048,512]{2,1,0:T(8,128)(2,1)} fusion(bf16[512,2048]{1,0:T(8,128)(2,1)} %bitcast.9, bf16[512,512]{1,0:T(8,128)(2,1)S(1)} %get-tuple-element.164), kind=kOutput, calls=%fused_computation.13 | convolution fusion | flops 1074790400 | bytes 4718592 | tf_op jit(solution)/shard_map/dot_general | solution.py:79
  201.4 4.3 %fusion.2 = bf16[1,512,2048]{2,1,0:T(8,128)(2,1)} fusion(bf16[512,2048]{1,0:T(8,128)(2,1)} %bitcast.11, f32[512,512]{1,0:T(8,128)S(1)} %copy-done.36, f32[512,512]{1,0:T(8,128)S(1)} %copy-done.35), kind=kOutput, calls=%fused_computation.15 | convolution fusion | flops 1076363264 | bytes 6291456 | tf_op jit(solution)/shard_map/dot_general | solution.py:76
  205.7 1.9 gather_fusion
  207.6 1.3 reshape.91
  209.6 8.9 %psum.7 = f32[128]{0:T(128)S(1)} all-reduce(f32[128]{0:T(128)S(1)} %multiply_reduce_fusion), channel_id=1, replica_groups=mesh['sp'=8,'tp'=4] {'tp'}, use_global_device_ids=true, to_apply=%region_8.9 | all-reduce | flops 128 | bytes 1024 | tf_op jit(solution)/shard_map/psum | solution.py:103
  218.6 1.0 add_convert_fusion.1
  219.6 11.0 %all_gather.17 = bf16[128,2048]{1,0:T(8,128)(2,1)S(1)} all-gather(bf16[128,512]{1,0:T(8,128)(2,1)S(1)} %add_convert_fusion.1), channel_id=1, replica_groups=mesh['sp'=8,'tp'=4] {'tp'}, dimensions={1}, use_global_device_ids=true | all-gather | bytes 655360 | tf_op jit(solution)/shard_map/all_gather | solution.py:107
  230.6 1.5 fusion.65
  242.3 1.4 add_multiply_fusion.4
  244.4 1.4 pad_maximum_fusion.6
  247.2 1.5 add_multiply_fusion
  249.4 0.9 pad_maximum_fusion.2
  250.3 0.9 pad.229
  251.2 2.2 pad.228
  253.4 1.2 fusion.51
  254.6 1.5 pad_maximum_fusion.1
  256.1 0.9 pad.200
  257.0 8.4 %all-gather = f32[8,1,256]{2,1,0:T(1,128)S(1)} all-gather(f32[1,1,256]{2,1,0:T(1,128)S(1)} %add_bitcast_fusion.1), channel_id=1, replica_groups=mesh['sp'=8,'tp'=4] {'sp'}, dimensions={0}, use_global_device_ids=true | all-gather | bytes 9216 | tf_op jit(solution)/shard_map/all_gather | solution.py:11
  265.5 1.5 convolution_convert_fusion.3
  267.1 4.3 %fusion.1 = bf16[1,2048,512]{2,1,0:T(8,128)(2,1)} fusion(bf16[512,2048]{1,0:T(8,128)(2,1)} %bitcast.9, bf16[512,512]{1,0:T(8,128)(2,1)S(1)} %copy-done.16), kind=kOutput, calls=%fused_computation.14 | convolution fusion | flops 1074790400 | bytes 4718592 | tf_op jit(solution)/shard_map/dot_general | solution.py:82
  271.6 14.8 %all-gather.2 = f32[8,1,256]{2,1,0:T(1,128)S(1)} all-gather(f32[1,1,256]{2,1,0:T(1,128)S(1)} %copy-done.31), channel_id=1, replica_groups=mesh['sp'=8,'tp'=4] {'sp'}, dimensions={0}, use_global_device_ids=true | all-gather | bytes 9216 | tf_op jit(solution)/shard_map/all_gather | solution.py:11
  286.4 8.7 %all-gather.3 = f32[8,1,256]{2,1,0:T(1,128)S(1)} all-gather(f32[1,1,256]{2,1,0:T(1,128)S(1)} %get-tuple-element.168), channel_id=1, replica_groups=mesh['sp'=8,'tp'=4] {'sp'}, dimensions={0}, use_global_device_ids=true | all-gather | bytes 9216 | tf_op jit(solution)/shard_map/all_gather | solution.py:11
  295.5 1.9 fusion.20
  298.1 5.4 %reduce-scatter.5.cloned.1.call-done = bf16[256,256]{1,0:T(8,128)(2,1)} async-done(((bf16[2048,256]{1,0:T(8,128)(2,1)}), bf16[256,256]{1,0:T(8,128)(2,1)}) %reduce-scatter.5.cloned.1.call-update) | async-done | bytes 131088 | tf_op jit(solution)/shard_map/reduce_scatter | solution.py:123
  303.4 1.6 convert_element_type.91
  (330 shorter events, 29.3 us)
Async XLA Ops:
  7.2 73.7 %copy-start = (bf16[1,2048,512]{2,1,0:T(8,128)(2,1)S(1)}, bf16[1,2048,512]{2,1,0:T(8,128)(2,1)}, u32[]{:S(2)}) copy-start(bf16[1,2048,512]{2,1,0:T(8,128)(2,1)} %param.25) | copy-start | bytes 6291460
  17.6 6.5 %copy-start.4 = (bf16[128,2048]{1,0:T(8,128)(2,1)S(1)}, bf16[128,2048]{1,0:T(8,128)(2,1)}, u32[]{:S(2)}) copy-start(bf16[128,2048]{1,0:T(8,128)(2,1)} %param.19) | copy-start | bytes 1572868
  17.6 55.6 %all-to-all-start = ((bf16[8,64,2048]{2,1,0:T(8,128)(2,1)}), bf16[8,64,2048]{2,1,0:T(8,128)(2,1)}, u32[]{:S(2)}, u32[]{:S(2)}) async-start(bf16[8,64,2048]{2,1,0:T(8,128)(2,1)} %bitcast.86), calls=%async_computation | async-start | bytes 4194304 | tf_op jit(solution)/shard_map/all_to_all | solution.py:63
  26.5 3.7 %copy-start.32 = (f32[128,2]{0,1:T(2,128)S(1)}, f32[128,2]{0,1:T(2,128)}, u32[]{:S(2)}) copy-start(f32[128,2]{0,1:T(2,128)} %param.24) | copy-start | bytes 3076
  73.2 4.8 %copy-start.33 = (f32[256]{0:T(256)S(1)}, f32[256]{0:T(256)}, u32[]{:S(2)}) copy-start(f32[256]{0:T(256)} %param.31) | copy-start | bytes 3076
  73.2 4.8 %copy-start.5 = (bf16[128,256]{1,0:T(8,128)(2,1)S(1)}, bf16[128,256]{1,0:T(8,128)(2,1)}, u32[]{:S(2)}) copy-start(bf16[128,256]{1,0:T(8,128)(2,1)} %param.30) | copy-start | bytes 196612
  73.2 4.8 %copy-start.17 = (f32[128,256]{1,0:T(8,128)S(1)}, f32[128,256]{1,0:T(8,128)}, u32[]{:S(2)}) copy-start(f32[128,256]{1,0:T(8,128)} %param.32) | copy-start | bytes 393220
  73.2 4.8 %copy-start.18 = (bf16[128,256]{1,0:T(8,128)(2,1)S(1)}, bf16[128,256]{1,0:T(8,128)(2,1)}, u32[]{:S(2)}) copy-start(bf16[128,256]{1,0:T(8,128)(2,1)} %param.28) | copy-start | bytes 196612
  73.2 4.8 %copy-start.20 = (bf16[128,256]{1,0:T(8,128)(2,1)S(1)}, bf16[128,256]{1,0:T(8,128)(2,1)}, u32[]{:S(2)}) copy-start(bf16[128,256]{1,0:T(8,128)(2,1)} %param.29) | copy-start | bytes 196612
  73.2 53.5 %all-to-all-start.1 = ((bf16[8,64,2048]{2,1,0:T(8,128)(2,1)}), bf16[8,64,2048]{2,1,0:T(8,128)(2,1)}, u32[]{:S(2)}, u32[]{:S(2)}) async-start(bf16[8,64,2048]{2,1,0:T(8,128)(2,1)} %bitcast.85), calls=%async_computation.1 | async-start | bytes 4194304 | tf_op jit(solution)/shard_map/all_to_all | solution.py:62
  77.8 92.1 %reduce-scatter.3.cloned.1.call-start = ((), (), s32[]{:S(2)}) async-start(), calls=%async_computation.5 | async-start | bytes 2621440 | tf_op jit(solution)/shard_map/reduce_scatter | solution.py:89
  78.1 6.8 %copy-start.28 = (f32[256]{0:T(256)}, f32[256]{0:T(256)S(1)}, u32[]{:S(2)}) copy-start(f32[256]{0:T(256)S(1)} %fusion.50) | copy-start | bytes 3076
  80.9 4.0 %copy-start.1 = (bf16[1,2048,512]{2,1,0:T(8,128)(2,1)S(1)}, bf16[1,2048,512]{2,1,0:T(8,128)(2,1)}, u32[]{:S(2)}) copy-start(bf16[1,2048,512]{2,1,0:T(8,128)(2,1)} %param.26) | copy-start | bytes 6291460
  131.2 1.3 copy-start.15
  131.2 1.8 copy-start.2
  135.6 0.8 copy-start.23
  135.6 0.9 copy-start.24
  136.4 1.4 copy-start.26
  136.4 1.4 copy-start.27
  137.8 32.0 %copy-start.7 = (f32[64,256]{1,0:T(8,128)}, f32[64,256]{1,0:T(8,128)S(1)}, u32[]{:S(2)}) copy-start(f32[64,256]{1,0:T(8,128)S(1)} %pad.198) | copy-start | bytes 196612
  138.6 36.6 %copy-start.8 = (f32[128,256]{1,0:T(8,128)}, f32[128,256]{1,0:T(8,128)S(1)}, u32[]{:S(2)}) copy-start(f32[128,256]{1,0:T(8,128)S(1)} %pad.186) | copy-start | bytes 393220
  169.8 35.9 %all-to-all-start.2 = ((bf16[8,64,512]{2,1,0:T(8,128)(2,1)}), bf16[8,64,512]{2,1,0:T(8,128)(2,1)S(1)}, u32[]{:S(2)}, u32[]{:S(2)}) async-start(bf16[8,64,512]{2,1,0:T(8,128)(2,1)} %bitcast.88), calls=%async_computation.3 | async-start | bytes 1048576 | tf_op jit(solution)/shard_map/all_to_all | solution.py:92
  174.4 129.0 %reduce-scatter.5.cloned.1.call-start = ((), (), s32[]{:S(2)}) async-start(), calls=%async_computation.6 | async-start | bytes 1179648 | tf_op jit(solution)/shard_map/reduce_scatter | solution.py:123
  197.1 4.4 %copy-start.35 = (f32[512,512]{1,0:T(8,128)S(1)}, f32[512,512]{1,0:T(8,128)}, u32[]{:S(2)}) copy-start(f32[512,512]{1,0:T(8,128)} %fusion.5) | copy-start | bytes 3145732
  197.1 4.4 %copy-start.36 = (f32[512,512]{1,0:T(8,128)S(1)}, f32[512,512]{1,0:T(8,128)}, u32[]{:S(2)}) copy-start(f32[512,512]{1,0:T(8,128)} %fusion.8) | copy-start | bytes 3145732
  205.7 3.8 %copy-start.3 = (bf16[128,2048]{1,0:T(8,128)(2,1)S(1)}, bf16[128,2048]{1,0:T(8,128)(2,1)}, u32[]{:S(2)}) copy-start(bf16[128,2048]{1,0:T(8,128)(2,1)} %param.20) | copy-start | bytes 1572868
  205.7 12.9 %copy-start.34 = (f32[128]{0:T(128)S(1)}, f32[128]{0:T(128)}, u32[]{:S(2)}) copy-start(f32[128]{0:T(128)} %param.21) | copy-start | bytes 1540
  219.6 12.8 %copy-start.21 = (f32[64,256]{1,0:T(8,128)S(1)}, f32[64,256]{1,0:T(8,128)}, u32[]{:S(2)}) copy-start(f32[64,256]{1,0:T(8,128)} %slice.526) | copy-start | bytes 196612
  219.6 12.8 %copy-start.22 = (f32[64,256]{1,0:T(8,128)S(1)}, f32[64,256]{1,0:T(8,128)}, u32[]{:S(2)}) copy-start(f32[64,256]{1,0:T(8,128)} %slice.519) | copy-start | bytes 196612
  232.4 14.8 %copy-start.25 = (f32[63,256]{1,0:T(8,128)S(1)}, f32[63,256]{1,0:T(8,128)}, u32[]{:S(2)}) copy-start(f32[63,256]{1,0:T(8,128)} %slice.517) | copy-start | bytes 193540
  239.1 17.8 %copy-start.11 = (f32[128,256]{1,0:T(8,128)S(1)}, f32[128,256]{1,0:T(8,128)}, u32[]{:S(2)}) copy-start(f32[128,256]{1,0:T(8,128)} %pad.201) | copy-start | bytes 393220
  239.4 26.1 %copy-start.9 = (f32[128,256]{1,0:T(8,128)S(1)}, f32[128,256]{1,0:T(8,128)}, u32[]{:S(2)}) copy-start(f32[128,256]{1,0:T(8,128)} %copy-done.8) | copy-start | bytes 393220
  239.4 26.1 %copy-start.10 = (f32[128,256]{1,0:T(8,128)S(1)}, f32[128,256]{1,0:T(8,128)}, u32[]{:S(2)}) copy-start(f32[128,256]{1,0:T(8,128)} %pad.187) | copy-start | bytes 393220
  240.9 8.5 %copy-start.30 = (f32[1,256]{1,0:T(1,128)S(1)}, f32[1,256]{1,0:T(1,128)}, u32[]{:S(2)}) copy-start(f32[1,256]{1,0:T(1,128)} %slice.636) | copy-start | bytes 3076
  251.2 14.3 %copy-start.12 = (f32[128,256]{1,0:T(8,128)}, f32[128,256]{1,0:T(8,128)S(1)}, u32[]{:S(2)}) copy-start(f32[128,256]{1,0:T(8,128)S(1)} %pad.229) | copy-start | bytes 393220
  265.5 1.5 copy-start.16
  267.0 4.4 %copy-start.13 = (f32[128,256]{1,0:T(8,128)S(1)}, f32[128,256]{1,0:T(8,128)}, u32[]{:S(2)}) copy-start(f32[128,256]{1,0:T(8,128)} %copy-done.12) | copy-start | bytes 393220
  267.0 4.4 %copy-start.14 = (f32[128,256]{1,0:T(8,128)S(1)}, f32[128,256]{1,0:T(8,128)}, u32[]{:S(2)}) copy-start(f32[128,256]{1,0:T(8,128)} %pad.228) | copy-start | bytes 393220
  267.0 4.6 %copy-start.31 = (f32[1,1,256]{2,1,0:T(1,128)S(1)}, f32[1,1,256]{2,1,0:T(1,128)}, u32[]{:S(2)}) copy-start(f32[1,1,256]{2,1,0:T(1,128)} %get-tuple-element.169) | copy-start | bytes 3076
  267.0 28.4 %copy-start.6 = (bf16[128,256]{1,0:T(8,128)(2,1)S(1)}, bf16[128,256]{1,0:T(8,128)(2,1)}, u32[]{:S(2)}) copy-start(bf16[128,256]{1,0:T(8,128)(2,1)} %param.30) | copy-start | bytes 196612
  267.0 28.4 %copy-start.19 = (bf16[128,256]{1,0:T(8,128)(2,1)S(1)}, bf16[128,256]{1,0:T(8,128)(2,1)}, u32[]{:S(2)}) copy-start(bf16[128,256]{1,0:T(8,128)(2,1)} %param.28) | copy-start | bytes 196612
  267.0 28.4 %copy-start.29 = (f32[256]{0:T(256)S(1)}, f32[256]{0:T(256)}, u32[]{:S(2)}) copy-start(f32[256]{0:T(256)} %copy-done.28) | copy-start | bytes 3076
Sparse Core Ops, SparseCore 0:
  135.7 34.0 reduce-scatter.2
  267.1 36.2 reduce-scatter.4
where the time goes:
time: 314 us; the launch traced here: 312 us
  waiting for transfers between devices  111 us (35%)
  blocking collectives  64.1 us (20%)
  local copies, waits for them, and re-layouts  45.8 us (15%)
  matrix products  32 us (10%)
  other arithmetic  27.3 us (9%)
  starting transfers between devices  15.9 us (5%)
  between operations  15.3 us (5%)
    all_gather x4, blocking collectives, carried_in(): gathered = jax.tree.map(lambda a: lax.all_gather(a, axis), part)  44.1 us
    all_to_all x1, waiting for transfers between devices, shards(): lax.all_to_all(grad_send, 'sp', split_axis=0, concat_axis=0, tiled=True)  38.1 us
    all_to_all x1, waiting for transfers between devices, shards(): lax.all_to_all(token_send, 'sp', split_axis=0, concat_axis=0, tiled=True)  38 us
    reduce_scatter x1, waiting for transfers between devices, shards(): lax.psum_scatter(partial_rows.astype(jnp.bfloat16), 'tp', scatter_dimensi...  29.9 us
    slice x49, local copies, waits for them, and re-layouts, shards(): lax.associative_scan(link, (keep_next, d_state), reverse=True, axis=0)  12.8 us
    all_gather x1, blocking collectives, shards(): d_mix = lax.all_gather(mix_part, 'tp', axis=1, tiled=True)  11 us
    psum x1, blocking collectives, shards(): stat = lax.psum(jnp.sum(gained * nhat, axis=1), 'tp')[:, None] / features  8.94 us
    all_to_all x1, starting transfers between devices, shards(): lax.all_to_all(token_send, 'sp', split_axis=0, concat_axis=0, tiled=True)  6.49 us
  transfers between devices with their start and end apart: 5, of which 4 were waited for; matrix products, arithmetic and copies ran while one was open for 16% of the time, Pallas kernels for 0%

commit v1 on v0

v1 whole, which is shorter than its diff:
```python
import functools

import jax
import jax.numpy as jnp
from jax import lax
from jax.experimental import pallas as pl
from jax.experimental.pallas import tpu as pltpu
from jax.sharding import PartitionSpec as P

MESH = pl.DeviceIdType.MESH
VMEM_LIMIT = 56 * 1024 * 1024


def greet(n, m, me, j):
    barrier = pltpu.get_barrier_semaphore()
    for k in range(1, n):
        pl.semaphore_signal(
            barrier, inc=1, device_id={"sp": lax.rem(me + k, n)}, device_id_type=MESH
        )
    for p in range(1, m):
        pl.semaphore_signal(
            barrier, inc=1, device_id={"tp": lax.rem(j + p, m)}, device_id_type=MESH
        )
    pl.semaphore_wait(barrier, n - 1 + m - 1)


def send(src, dst, send_sem, recv_sem, where):
    return pltpu.make_async_remote_copy(
        src_ref=src,
        dst_ref=dst,
        send_sem=send_sem,
        recv_sem=recv_sem,
        device_id=where,
        device_id_type=MESH,
    )


def scan_rows(a, b, reverse):
    rows = a.shape[0]
    place = lax.broadcasted_iota(jnp.int32, a.shape, 0)
    step = 1
    while step < rows:
        if reverse:
            known = place < rows - step
            shift = rows - step
        else:
            known = place >= step
            shift = step
        a_far = jnp.where(known, pltpu.roll(a, shift, 0), 1.0)
        b_far = jnp.where(known, pltpu.roll(b, shift, 0), 0.0)
        b = a * b_far + b
        a = a * a_far
        step *= 2
    return a, b


def dispatch_kernel(
    n, m, xs, ys, keep, driven, xo, yo, hidden, prev, carry,
    cum, loc, s1s, s1r, s2s, s2r, cs, cr, lsem,
):
    me, j = lax.axis_index("sp"), lax.axis_index("tp")
    cap, q = xs.shape[0] // n, xs.shape[1]
    tok = keep.shape[0]
    rows = lambda s: pl.ds(pl.multiple_of(s * cap, cap), cap)
    cols = lambda t: pl.ds(pl.multiple_of(t * q, q), q)
    pairs = ((0, xs, xo), (1, ys, yo))
    a, b = scan_rows(keep[...], driven[...], False)
    cum[...] = a
    loc[...] = b
    width = a.shape[1]
    carry[me] = jnp.concatenate(
        [a[tok - 1 : tok], b[tok - 1 : tok], jnp.zeros((6, width), jnp.float32)], axis=0
    )
    greet(n, m, me, j)

    def first(k):
        to = lax.rem(me + k, n)
        return [
            send(s.at[rows(to)], o.at[rows(me), cols(j)], s1s.at[i], s1r.at[i, k], {"sp": to})
            for i, s, o in pairs
        ]

    def carried(k):
        to = lax.rem(me + k, n)
        return send(carry.at[me], carry.at[me], cs.at[k], cr.at[k], {"sp": to})

    own = [
        pltpu.make_async_copy(s.at[rows(me)], o.at[rows(me), cols(j)], lsem.at[i])
        for i, s, o in pairs
    ]
    for c in own:
        c.start()

    def start_carry(k, _):
        carried(k).start()
        return 0

    lax.fori_loop(1, n, start_carry, 0)

    def start_first(k, _):
        for c in first(k):
            c.start()
        return 0

    lax.fori_loop(1, n, start_first, 0)

    def forward(source):
        for p in range(1, m):
            for i, _, o in pairs:
                block = o.at[rows(source), cols(j)]
                send(block, block, s2s.at[i, p], s2r.at[i, p], {"tp": lax.rem(j + p, m)}).start()

    for c in own:
        c.wait()
    forward(me)

    def relay(k, _):
        source = lax.rem(me - k + n, n)
        for i, s, o in pairs:
            block = o.at[rows(source), cols(j)]
            send(block, block, s1s.at[i], s1r.at[i, k], {"sp": source}).wait_recv()
        forward(source)
        return 0

    lax.fori_loop(1, n, relay, 0)

    def take_carry(k, _):
        source = lax.rem(me - k + n, n)
        send(carry.at[source], carry.at[source], cs.at[k], cr.at[k], {"sp": source}).wait_recv()
        carried(k).wait_send()
        return 0

    lax.fori_loop(1, n, take_carry, 0)
    state = jnp.zeros((1, width), jnp.float32)
    for s in range(n):
        state = jnp.where(s < me, carry[s, 0:1] * state + carry[s, 1:2], state)
    whole = loc[...] + cum[...] * state
    hidden[...] = whole.astype(hidden.dtype)
    place = lax.broadcasted_iota(jnp.int32, whole.shape, 0)
    prev[...] = jnp.where(place >= 1, pltpu.roll(whole, 1, 0), state)
    for i, s, o in pairs:
        part = s.at[pl.ds(0, (n - 1) * cap)]
        send(part, part, s1s.at[i], s1r.at[i, 0], {"sp": lax.rem(me + 1, n)}).wait_send()
        for p in range(1, m):
            far = lax.rem(j - p + m, m)
            mine, theirs = o.at[:, cols(j)], o.at[:, cols(far)]
            send(mine, mine, s2s.at[i, p], s2r.at[i, p], {"tp": far}).wait_send()
            send(theirs, theirs, s2s.at[i, p], s2r.at[i, p], {"tp": far}).wait_recv()


def return_kernel(
    n, m, pr, pick, hid, out, hid_all,
    stage, red, back, rs, rr, bs, br, gs, gr, hs, hr, lsem,
):
    me, j = lax.axis_index("sp"), lax.axis_index("tp")
    tok = hid.shape[0]
    cap, q = pr.shape[0] // n, pr.shape[1] // m
    rows = lambda s: pl.ds(pl.multiple_of(s * cap, cap), cap)
    cols = lambda t: pl.ds(pl.multiple_of(t * q, q), q)
    greet(n, m, me, j)
    own = pltpu.make_async_copy(hid, hid_all.at[me], lsem)
    own.start()

    def spread(k, _):
        to = lax.rem(me + k, n)
        for p in range(1, m):
            far = lax.rem(j + p, m)
            send(
                pr.at[rows(to), cols(far)],
                stage.at[p - 1, rows(to)],
                rs.at[k],
                rr.at[k],
                {"tp": far},
            ).start()
        return 0

    lax.fori_loop(1, n + 1, spread, 0)

    def share(k, _):
        to = lax.rem(me + k, n)
        send(hid, hid_all.at[me], hs.at[k], hr.at[k], {"sp": to}).start()
        return 0

    lax.fori_loop(1, n, share, 0)

    def ship(k):
        to = lax.rem(me + k, n)
        return send(red.at[rows(to)], back.at[rows(me)], bs.at[k], br.at[k], {"sp": to})

    def reduce(k, _):
        to = lax.rem(me + k, n)
        block = stage.at[:, rows(to)]
        got = send(block, block, rs.at[k], rr.at[k], {"tp": lax.rem(j + 1, m)})
        got.wait_recv()
        got.wait_send()
        total = pr[rows(to), cols(j)].astype(jnp.float32)
        for p in range(1, m):
            total = total + stage[p - 1, rows(to)].astype(jnp.float32)
        red[rows(to)] = total.astype(red.dtype)

        @pl.when(k > 1)
        def _():
            ship(k - 1).start()

        return 0

    lax.fori_loop(1, n + 1, reduce, 0)
    back[rows(me)] = red[rows(me)]

    def collect(k, _):
        source = lax.rem(me - k + n, n)
        block = back.at[rows(source)]
        send(block, block, bs.at[k], br.at[k], {"sp": source}).wait_recv()
        return 0

    lax.fori_loop(1, n, collect, 0)
    total = jnp.dot(pick[...], back[...], preferred_element_type=jnp.float32)
    out[:, cols(j)] = total.astype(out.dtype)

    def finish(k, _):
        source = lax.rem(me - k + n, n)
        ship(k).wait_send()
        got = send(hid, hid_all.at[source], hs.at[k], hr.at[k], {"sp": source})
        got.wait_recv()
        got.wait_send()
        return 0

    lax.fori_loop(1, n, finish, 0)
    own.wait()
    mine = out.at[:, cols(j)]
    for p in range(1, m):
        send(mine, mine, gs.at[p], gr.at[p], {"tp": lax.rem(j + p, m)}).start()
    for p in range(1, m):
        far = lax.rem(j - p + m, m)
        theirs = out.at[:, cols(far)]
        send(mine, mine, gs.at[p], gr.at[p], {"tp": far}).wait_send()
        send(theirs, theirs, gs.at[p], gr.at[p], {"tp": far}).wait_recv()


def last_kernel(
    n, m, mix_t, hid_all, d_state, keep, carry, total, gow,
    got, cum, loc, back, ms, mr, cs, cr, lsem,
):
    me, j = lax.axis_index("sp"), lax.axis_index("tp")
    tok, width = keep.shape
    slab = mix_t.shape[0] // n
    rows = lambda s: pl.ds(pl.multiple_of(s * slab, slab), slab)
    greet(n, m, me, j)
    own = pltpu.make_async_copy(mix_t.at[rows(me)], got.at[me], lsem)
    own.start()

    def blocks(k):
        to = lax.rem(me + k, n)
        return send(mix_t.at[rows(to)], got.at[me], ms.at[k], mr.at[k], {"sp": to})

    def carried(k):
        to = lax.rem(me + k, n)
        return send(back.at[me], back.at[me], cs.at[k], cr.at[k], {"sp": to})

    place = lax.broadcasted_iota(jnp.int32, (tok, width), 0)
    here = keep[...]
    after = jnp.where(place < tok - 1, pltpu.roll(here, tok - 1, 0), 1.0)
    a, b = scan_rows(after, d_state[...], True)
    cum[...] = a
    loc[...] = b
    back[me] = jnp.broadcast_to(here[0:1] * b[0:1], (8, width))
    own.wait()

    def start(k, _):
        carried(k).start()
        return 0

    lax.fori_loop(1, n, start, 0)

    def start_blocks(k, _):
        blocks(k).start()
        return 0

    lax.fori_loop(1, n, start_blocks, 0)

    def take(k, _):
        source = lax.rem(me - k + n, n)
        send(back.at[source], back.at[source], cs.at[k], cr.at[k], {"sp": source}).wait_recv()
        carried(k).wait_send()
        return 0

    lax.fori_loop(1, n, take, 0)
    enter = jnp.zeros((1, width), jnp.float32)
    for s in range(n - 1, -1, -1):
        enter = jnp.where(s > me, carry[s, 0:1] * enter + back[s, 0:1], enter)
    total[...] = loc[...] + cum[...] * enter
    gow[...] = jnp.dot(got[me], hid_all[me], preferred_element_type=jnp.float32)

    def add(k, _):
        source = lax.rem(me - k + n, n)
        send(got.at[source], got.at[source], ms.at[k], mr.at[k], {"sp": source}).wait_recv()
        blocks(k).wait_send()
        gow[...] += jnp.dot(got[source], hid_all[source], preferred_element_type=jnp.float32)
        return 0

    lax.fori_loop(1, n, add, 0)


def call(kernel, n, m, outs, scratch, ident, *args):
    return pl.pallas_call(
        functools.partial(kernel, n, m),
        out_shape=tuple(jax.ShapeDtypeStruct(s, d) for s, d in outs),
        in_specs=[pl.BlockSpec(memory_space=pltpu.VMEM)] * len(args),
        out_specs=tuple(pl.BlockSpec(memory_space=pltpu.VMEM) for _ in outs),
        scratch_shapes=scratch,
        compiler_params=pltpu.CompilerParams(
            collective_id=ident, has_side_effects=True, vmem_limit_bytes=VMEM_LIMIT
        ),
    )(*args)


def shards(
    cotangent,
    normed,
    inverse_root_mean_square,
    expert_norm_scale,
    routes,
    route_probability_weight,
    gate_weight,
    up_weight,
    down_weight,
    recurrence_input,
    recurrence_gate_logits,
    input_gate_logits,
    channel_decay_weight,
    extra_log_decay,
    output_matrix,
):
    tok_rows, features = normed.shape
    n, m = lax.axis_size("sp"), lax.axis_size("tp")
    picks = routes.shape[1]
    capacity = 2 * picks * tok_rows // n
    slots = n * capacity
    q = features // m
    channels = recurrence_input.shape[1]
    f32, bf16 = jnp.float32, jnp.bfloat16
    dma = pltpu.SemaphoreType.DMA
    rowdims = (((0,), (0,)), ((), ()))
    coldims = (((1,), (1,)), ((), ()))

    chosen = routes.reshape(-1)
    member = chosen[:, None] == jnp.arange(n, dtype=jnp.int32)[None, :]
    order = jnp.arange(chosen.shape[0])
    below = (order[:, None] > order[None, :]).astype(bf16)
    before = jnp.dot(below, member.astype(bf16), preferred_element_type=f32)
    ranking = jnp.sum(jnp.where(member, before, 0.0), axis=1).astype(jnp.int32)
    landing = (chosen * capacity + ranking).reshape(tok_rows, picks)
    slot = jnp.arange(slots, dtype=jnp.int32)
    hits = [slot[:, None] == landing[:, k][None, :] for k in range(picks)]
    place = functools.reduce(jnp.logical_or, hits).astype(bf16)
    pick = functools.reduce(
        jnp.logical_or, [landing[:, k][:, None] == slot[None, :] for k in range(picks)]
    ).astype(bf16)
    share = sum(
        jnp.sum(jnp.where(h, route_probability_weight[:, k][None, :], 0.0), axis=1)
        for k, h in enumerate(hits)
    )
    offset = lax.axis_index("tp") * q
    normed_part = lax.dynamic_slice_in_dim(normed, offset, q, 1)
    cot_part = lax.dynamic_slice_in_dim(cotangent, offset, q, 1)
    token_send = jnp.dot(place, normed_part, preferred_element_type=f32).astype(bf16)
    grad_send = (
        share[:, None] * jnp.dot(place, cot_part, preferred_element_type=f32)
    ).astype(bf16)

    retention_factor = jax.nn.sigmoid(recurrence_gate_logits.astype(f32))
    admit = jax.nn.sigmoid(input_gate_logits.astype(f32))
    signal = recurrence_input.astype(f32)
    decay_speed = jax.nn.softplus(-channel_decay_weight)
    log_retention = -8.0 * retention_factor * decay_speed[None, :] + extra_log_decay
    keep = jnp.exp(log_retention)
    scale_in = jnp.sqrt(-jnp.expm1(2.0 * log_retention))
    driven = scale_in * admit * signal

    token_recv, grad_recv, hidden, state_prev, carry = call(
        dispatch_kernel, n, m,
        [
            ((slots, features), bf16),
            ((slots, features), bf16),
            ((tok_rows, channels), bf16),
            ((tok_rows, channels), f32),
            ((n, 8, channels), f32),
        ],
        [
            pltpu.VMEM((tok_rows, channels), f32),
            pltpu.VMEM((tok_rows, channels), f32),
            dma((2,)),
            dma((2, n)),
            dma((2, m)),
            dma((2, m)),
            dma((n,)),
            dma((n,)),
            dma((2,)),
        ],
        0, token_send, grad_send, keep, driven,
    )

    gate_w = gate_weight[0]
    up_w = up_weight[0]
    down_w = down_weight[0]
    gate_pre = jnp.dot(token_recv, gate_w, preferred_element_type=f32)
    up_pre = jnp.dot(token_recv, up_w, preferred_element_type=f32)
    sigma = jax.nn.sigmoid(gate_pre)
    swish = gate_pre * sigma
    active = (swish * up_pre).astype(bf16)
    d_active = lax.dot_general(grad_recv, down_w, coldims, preferred_element_type=f32)
    d_gate = (d_active * up_pre * sigma * (1.0 + gate_pre * (1.0 - sigma))).astype(bf16)
    d_up = (d_active * swish).astype(bf16)
    grad_down = lax.dot_general(active, grad_recv, rowdims, preferred_element_type=f32).astype(bf16)
    grad_gate = lax.dot_general(token_recv, d_gate, rowdims, preferred_element_type=f32).astype(bf16)
    grad_up = lax.dot_general(token_recv, d_up, rowdims, preferred_element_type=f32).astype(bf16)
    partial_rows = lax.dot_general(d_gate, gate_w, coldims, preferred_element_type=f32)
    partial_rows = partial_rows + lax.dot_general(d_up, up_w, coldims, preferred_element_type=f32)

    d_norm, hidden_all = call(
        return_kernel, n, m,
        [((tok_rows, features), bf16), ((n, tok_rows, channels), bf16)],
        [
            pltpu.VMEM((m - 1, slots, q), bf16),
            pltpu.VMEM((slots, q), bf16),
            pltpu.VMEM((slots, q), bf16),
            dma((n + 1,)),
            dma((n + 1,)),
            dma((n,)),
            dma((n,)),
            dma((m,)),
            dma((m,)),
            dma((n,)),
            dma((n,)),
            dma,
        ],
        1, partial_rows.astype(bf16), pick, hidden,
    )
    d_norm = d_norm.astype(f32)
    nhat = normed.astype(f32) / expert_norm_scale[None, :]
    gained = expert_norm_scale[None, :] * d_norm
    stat = jnp.mean(gained * nhat, axis=1, keepdims=True)
    d_mix = (
        cotangent.astype(f32) + inverse_root_mean_square[:, None] * (gained - nhat * stat)
    ).astype(bf16)
    d_state = jnp.dot(d_mix, output_matrix, preferred_element_type=f32)

    total, grad_out_weight = call(
        last_kernel, n, m,
        [((tok_rows, channels), f32), ((features // n, channels), f32)],
        [
            pltpu.VMEM((n, features // n, tok_rows), bf16),
            pltpu.VMEM((tok_rows, channels), f32),
            pltpu.VMEM((tok_rows, channels), f32),
            pltpu.VMEM((n, 8, channels), f32),
            dma((n,)),
            dma((n,)),
            dma((n,)),
            dma((n,)),
            dma,
        ],
        2, d_mix.T, hidden_all, d_state, keep, carry,
    )
    grad_rec_input = total * scale_in * admit
    grad_input_gate = total * scale_in * signal * admit * (1.0 - admit)
    d_log = total * state_prev * keep - total * admit * signal * keep * keep / scale_in
    grad_decay_gate = (
        d_log * (-8.0 * decay_speed[None, :]) * retention_factor * (1.0 - retention_factor)
    )
    return (
        grad_gate[None],
        grad_up[None],
        grad_down[None],
        grad_out_weight,
        grad_rec_input,
        grad_decay_gate,
        grad_input_gate,
    )


def solution(mesh):
    return jax.shard_map(
        shards,
        mesh=mesh,
        in_specs=(
            P("sp", None),
            P("sp", None),
            P("sp"),
            P(),
            P("sp", None),
            P("sp", None),
            P("sp", None, "tp"),
            P("sp", None, "tp"),
            P("sp", "tp", None),
            P("sp", "tp"),
            P("sp", "tp"),
            P("sp", "tp"),
            P("tp"),
            P("sp", "tp"),
            P(None, "tp"),
        ),
        out_specs=(
            P("sp", None, "tp"),
            P("sp", None, "tp"),
            P("sp", "tp", None),
            P("sp", "tp"),
            P("sp", "tp"),
            P("sp", "tp"),
            P("sp", "tp"),
        ),
        check_vma=False,
    )
```

time: 314 us -> 158 us (0.50)
  Pallas kernels: 0 us -> 116 us
  waiting for transfers between devices: 111 us -> 0 us
  blocking collectives: 64.1 us -> 0 us
  local copies, waits for them, and re-layouts: 45.8 us -> 8.37 us
  other arithmetic: 27.3 us -> 8 us
  starting transfers between devices: 15.9 us -> 0 us
  between operations: 15.3 us -> 0.95 us
  matrix products: 32 us -> 23 us
    pallas_call x0 -> x3, Pallas kernels: none -> 116 us  [call(): pl.pallas_call(functools.partial(kernel, n, m), out_shape=tuple((jax.Shap...]
    all_to_all x3 -> x0, waiting for transfers between devices: 76.1 us -> none  [the longest x1 38.1 us: shards(): lax.all_to_all(grad_send, 'sp', split_axis=0, concat_axis=0, tiled=True)]
    all_gather x5 -> x0, blocking collectives: 55.1 us -> none  [the longest x4 44.1 us: carried_in(): gathered = jax.tree.map(lambda a: lax.all_gather(a, axis), part)]
    reduce_scatter x2 -> x0, waiting for transfers between devices: 35.3 us -> none  [the longest x1 29.9 us: shards(): lax.psum_scatter(partial_rows.astype(jnp.bfloat16), 'tp', scatter_dimensi...]
    slice x94 -> x0, local copies, waits for them, and re-layouts: 16.2 us -> none  [the longest x49 12.8 us: shards(): lax.associative_scan(link, (keep_next, d_state), reverse=True, axis=0)]
    all_to_all x3 -> x0, starting transfers between devices: 15.6 us -> none  [the longest x1 6.49 us: shards(): lax.all_to_all(token_send, 'sp', split_axis=0, concat_axis=0, tiled=True)]
    dot_general x10 -> x12, matrix products: 32 us -> 23 us  [the longest x1 2.98 us: shards(): gate_pre = jnp.dot(token_recv, gate_w, preferred_element_type=f32)]
    psum x1 -> x0, blocking collectives: 8.94 us -> none  [shards(): stat = lax.psum(jnp.sum(gained * nhat, axis=1), 'tp')[:, None] / features]
  transfers between devices with their start and end apart: 5 -> 0, of which waited for: 4 -> 0; matrix products, arithmetic and copies ran while one was open for 16% -> 0% of each run, Pallas kernels for 0% -> 0%
where the time goes in v1:
time: 158 us; the launch traced here: 157 us
  Pallas kernels  116 us (73%)
  matrix products  23 us (15%)
  local copies, waits for them, and re-layouts  8.37 us (5%)
  other arithmetic  8 us (5%)
    pallas_call x3, Pallas kernels, call(): pl.pallas_call(functools.partial(kernel, n, m), out_shape=tuple((jax.Shap...  116 us
    unnamed x34, local copies, waits for them, and re-layouts  5.96 us

profile of v1, /device:TPU:0, one launch (start us, length us, event | category | flops | bytes accessed | tf_op | source)
XLA Modules:
  0.0 156.8 jit_solution(10136964814298083322)
XLA Ops:
  0.6 0.0 copy-start
  0.7 0.9 copy.43
  1.6 0.1 eq.72
  1.7 0.2 fusion.13
  1.9 0.1 convert_element_type.62
  2.1 0.1 copy.44
  2.1 0.7 multiply_add_fusion.1
  2.9 2.0 %convolution_convert_fusion.3.xs = bf16[512,512]{1,0:T(8,128)(2,1)} fusion(bf16[128,2048]{1,0:T(8,128)(2,1)} %param.16, s32[]{:T(128)S(6)} %select_n.20, s32[128]{0:T(128)S(1)} %get-tuple-element.35, s32[128]{0:T(128)S(1)} %get-tuple-element.34), kind=kOutput, calls=%fused_computation.18 | convolution fusion | flops 67567616 | bytes 656388 | tf_op jit(solution)/shard_map/dot_general | solution.py:366
  4.9 0.8 slice_bitcast_fusion
  5.6 0.2 select_reduce_fusion
  5.8 2.0 %fusion.12.ys = bf16[512,512]{1,0:T(8,128)(2,1)} fusion(f32[512]{0:T(512)S(1)} %add.42, bf16[128,2048]{1,0:T(8,128)(2,1)} %param.15, s32[]{:T(128)S(6)} %select_n.20, s32[128]{0:T(128)S(1)} %get-tuple-element.35, s32[128]{0:T(128)S(1)} %get-tuple-element.34), kind=kOutput, calls=%fused_computation.17 | convolution fusion | flops 67829760 | bytes 658436 | tf_op jit(solution)/shard_map/dot_general | solution.py:368
  7.8 0.7 fusion.37
  8.5 1.8 %convert_multiply_fusion.3 = (f32[128,256]{1,0:T(8,128)}, f32[128,256]{1,0:T(8,128)}) fusion(bf16[128,256]{1,0:T(8,128)(2,1)} %param.24, bf16[128,256]{1,0:T(8,128)(2,1)} %param.26, f32[128,256]{1,0:T(8,128)} %param.28, f32[256]{0:T(256)S(1)} %fusion.37, bf16[128,256]{1,0:T(8,128)(2,1)} %param.25), kind=kLoop, calls=%fused_computation.43 | loop fusion | flops 491520 | bytes 590848 | tf_op jit(solution)/shard_map/mul | solution.py:378
  10.4 57.0 %shard_map.198 = (bf16[512,2048]{1,0:T(8,128)(2,1)}, bf16[512,2048]{1,0:T(8,128)(2,1)}, bf16[128,256]{1,0:T(8,128)(2,1)}, f32[128,256]{1,0:T(8,128)}, f32[8,8,256]{2,1,0:T(8,128)}) custom-call(bf16[512,512]{1,0:T(8,128)(2,1)} %convolution_convert_fusion.3.xs, bf16[512,512]{1,0:T(8,128)(2,1)} %fusion.12.ys, f32[128,256]{1,0:T(8,128)} %get-tuple-element.31.keep, ...), custom_call_target="tpu_custom_call" | custom-call | tf_op jit(solution)/shard_map/pallas_call | solution.py:305
  67.4 0.0 copy-done
  67.4 0.0 copy-start.2
  67.4 3.0 %fusion.5 = f32[512,512]{1,0:T(8,128)S(1)} fusion(bf16[512,2048]{1,0:T(8,128)(2,1)} %get-tuple-element.16, bf16[1,2048,512]{2,1,0:T(8,128)(2,1)S(1)} %copy-done), kind=kOutput, calls=%fused_computation.9 | convolution fusion | flops 1073741824 | bytes 5242880 | tf_op jit(solution)/shard_map/dot_general | solution.py:406
  70.4 0.0 copy-start.12
  70.4 1.2 fusion.8
  71.7 0.3 copy-done.12
  72.0 0.6 copy-done.13
  72.7 1.7 %multiply_convert_fusion.1 = (bf16[512,512]{1,0:T(8,128)(2,1)S(1)}, bf16[512,512]{1,0:T(8,128)(2,1)S(1)}) fusion(f32[512,512]{1,0:T(8,128)S(1)} %fusion.5, f32[512,512]{1,0:T(8,128)S(1)} %fusion.8, bf16[512,2048]{1,0:T(8,128)(2,1)S(1)} %copy-done.13, bf16[1,512,2048]{2,1,0:T(8,128)(2,1)S(1)} %copy-done.12), kind=kOutput, calls=%fused_computation.26 | convolution fusion | flops 1077149696 | bytes 7340032 | tf_op jit(solution)/shard_map/dot_general | solution.py:411
  74.3 2.6 %fusion = bf16[1,2048,512]{2,1,0:T(8,128)(2,1)} fusion(bf16[512,2048]{1,0:T(8,128)(2,1)S(1)} %copy-done.14, bf16[512,512]{1,0:T(8,128)(2,1)S(1)} %get-tuple-element.26), kind=kOutput, calls=%fused_computation.4 | convolution fusion | flops 1074790400 | bytes 4718592 | tf_op jit(solution)/shard_map/dot_general | solution.py:415
  77.0 2.6 %fusion.1 = bf16[1,2048,512]{2,1,0:T(8,128)(2,1)} fusion(bf16[512,2048]{1,0:T(8,128)(2,1)S(1)} %copy-done.14, bf16[512,512]{1,0:T(8,128)(2,1)S(1)} %get-tuple-element.25), kind=kOutput, calls=%fused_computation.5 | convolution fusion | flops 1074790400 | bytes 4718592 | tf_op jit(solution)/shard_map/dot_general | solution.py:416
  79.6 2.7 %fusion.2 = bf16[1,512,2048]{2,1,0:T(8,128)(2,1)} fusion(bf16[512,2048]{1,0:T(8,128)(2,1)S(1)} %copy-done.13, f32[512,512]{1,0:T(8,128)S(1)} %fusion.8, f32[512,512]{1,0:T(8,128)S(1)} %fusion.5), kind=kOutput, calls=%fused_computation.6 | convolution fusion | flops 1076363264 | bytes 6291456 | tf_op jit(solution)/shard_map/dot_general | solution.py:414
  82.3 1.3 fusion.3
  83.6 2.6 %add_convert_fusion.pr = bf16[512,2048]{1,0:T(8,128)(2,1)} fusion(f32[512,2048]{1,0:T(8,128)S(1)} %fusion.3, bf16[512,512]{1,0:T(8,128)(2,1)S(1)} %get-tuple-element.25, bf16[1,2048,512]{2,1,0:T(8,128)(2,1)S(1)} %copy-done.2), kind=kOutput, calls=%fused_computation | convolution fusion | flops 1075838976 | bytes 8912896 | tf_op jit(solution)/shard_map/dot_general | solution.py:418
  86.2 0.8 fusion.17.pick
  87.0 43.4 %shard_map.199 = (bf16[128,2048]{1,0:T(8,128)(2,1)}, bf16[8,128,256]{2,1,0:T(8,128)(2,1)}) custom-call(bf16[512,2048]{1,0:T(8,128)(2,1)} %add_convert_fusion.pr, bf16[128,512]{1,0:T(8,128)(2,1)} %fusion.17.pick, bf16[128,256]{1,0:T(8,128)(2,1)} %get-tuple-element.18.hid), custom_call_target="tpu_custom_call" | custom-call | tf_op jit(solution)/shard_map/pallas_call | solution.py:305
  130.4 0.0 copy-start.10
  130.4 0.0 copy-start.11
  130.4 1.3 copy.46
  131.8 1.0 copy.45
  132.8 1.3 copy.47
  134.1 0.0 copy-done.10
  134.1 0.0 copy-start.3
  134.1 0.4 multiply_reduce_fusion
  134.5 0.0 copy-start.5
  134.5 0.0 copy-start.6
  134.5 0.0 copy-start.7
  134.5 0.0 copy-start.8
  134.5 1.5 add_convert_fusion.1
  136.1 0.0 copy-start.1
  136.1 0.0 copy-done.3
  136.1 1.0 fusion.42.d_state
  137.1 16.1 %shard_map.200 = (f32[128,256]{1,0:T(8,128)}, f32[256,256]{1,0:T(8,128)}) custom-call(bf16[2048,128]{1,0:T(8,128)(2,1)} %bitcast.42, bf16[8,128,256]{2,1,0:T(8,128)(2,1)} %get-tuple-element.20.hid_all, f32[128,256]{1,0:T(8,128)} %fusion.42.d_state, f32[128,256]{1,0:T(8,128)} %get-tuple-element.31.keep, f32[8,8,256]{2,1,0:T(8,128)} %get-tuple-element.21.carry), custom_call_target="tpu_custom_call" | custom-call | tf_op jit(solution)/shard_map/pallas_call | solution.py:305
  153.3 1.9 %fusion.22 = (f32[128,256]{1,0:T(8,128)}, f32[128,256]{1,0:T(8,128)}, f32[128,256]{1,0:T(8,128)}) fusion(bf16[128,256]{1,0:T(8,128)(2,1)S(1)} %copy-done.6, f32[128,256]{1,0:T(8,128)} %get-tuple-element.23, bf16[128,256]{1,0:T(8,128)(2,1)S(1)} %copy-done.7, f32[128,256]{1,0:T(8,128)S(1)} %copy-done.5, f32[256]{0:T(256)S(1)} %fusion.37, ...), kind=kLoop, calls=%fused_computation.45 | loop fusion | flops 1015808 | bytes 984064 | tf_op jit(solution)/shard_map/mul | solution.py:465
  155.1 1.7 %copy.49 = f32[256,256]{1,0:T(8,128)} copy(f32[256,256]{1,0:T(8,128)} %get-tuple-element.48) | data formatting | bytes 524288
  (18 shorter events, 0.1 us)
Async XLA Ops:
  0.6 66.8 %copy-start = (bf16[1,2048,512]{2,1,0:T(8,128)(2,1)S(1)}, bf16[1,2048,512]{2,1,0:T(8,128)(2,1)}, u32[]{:S(2)}) copy-start(bf16[1,2048,512]{2,1,0:T(8,128)(2,1)} %param.21) | copy-start | bytes 6291460
  67.4 3.0 %copy-start.2 = (bf16[1,2048,512]{2,1,0:T(8,128)(2,1)S(1)}, bf16[1,2048,512]{2,1,0:T(8,128)(2,1)}, u32[]{:S(2)}) copy-start(bf16[1,2048,512]{2,1,0:T(8,128)(2,1)} %param.22) | copy-start | bytes 6291460
  67.4 3.0 %copy-start.14 = (bf16[512,2048]{1,0:T(8,128)(2,1)S(1)}, bf16[512,2048]{1,0:T(8,128)(2,1)}, u32[]{:S(2)}) copy-start(bf16[512,2048]{1,0:T(8,128)(2,1)} %get-tuple-element.16) | copy-start | bytes 6291460
  70.4 1.6 %copy-start.12 = (bf16[1,512,2048]{2,1,0:T(8,128)(2,1)S(1)}, bf16[1,512,2048]{2,1,0:T(8,128)(2,1)}, u32[]{:S(2)}) copy-start(bf16[1,512,2048]{2,1,0:T(8,128)(2,1)} %param.23) | copy-start | bytes 6291460
  70.4 2.2 %copy-start.13 = (bf16[512,2048]{1,0:T(8,128)(2,1)S(1)}, bf16[512,2048]{1,0:T(8,128)(2,1)}, u32[]{:S(2)}) copy-start(bf16[512,2048]{1,0:T(8,128)(2,1)} %get-tuple-element.17) | copy-start | bytes 6291460
  86.2 45.5 %copy-start.4 = (bf16[128,2048]{1,0:T(8,128)(2,1)S(1)}, bf16[128,2048]{1,0:T(8,128)(2,1)}, u32[]{:S(2)}) copy-start(bf16[128,2048]{1,0:T(8,128)(2,1)} %param.15) | copy-start | bytes 1572868
  130.4 3.7 %copy-start.10 = (f32[2048]{0:T(1024)S(1)}, f32[2048]{0:T(1024)}, u32[]{:S(2)}) copy-start(f32[2048]{0:T(1024)} %param.18) | copy-start | bytes 24580
  130.4 4.1 %copy-start.11 = (f32[128]{0:T(128)S(1)}, f32[128]{0:T(128)}, u32[]{:S(2)}) copy-start(f32[128]{0:T(128)} %param.17) | copy-start | bytes 1540
  134.1 2.0 %copy-start.3 = (bf16[2048,256]{1,0:T(8,128)(2,1)S(1)}, bf16[2048,256]{1,0:T(8,128)(2,1)}, u32[]{:S(2)}) copy-start(bf16[2048,256]{1,0:T(8,128)(2,1)} %param.29) | copy-start | bytes 3145732
  134.5 18.7 %copy-start.5 = (f32[128,256]{1,0:T(8,128)S(1)}, f32[128,256]{1,0:T(8,128)}, u32[]{:S(2)}) copy-start(f32[128,256]{1,0:T(8,128)} %param.28) | copy-start | bytes 393220
  134.5 18.7 %copy-start.6 = (bf16[128,256]{1,0:T(8,128)(2,1)S(1)}, bf16[128,256]{1,0:T(8,128)(2,1)}, u32[]{:S(2)}) copy-start(bf16[128,256]{1,0:T(8,128)(2,1)} %param.24) | copy-start | bytes 196612
  134.5 18.7 %copy-start.7 = (bf16[128,256]{1,0:T(8,128)(2,1)S(1)}, bf16[128,256]{1,0:T(8,128)(2,1)}, u32[]{:S(2)}) copy-start(bf16[128,256]{1,0:T(8,128)(2,1)} %param.26) | copy-start | bytes 196612
  134.5 18.7 %copy-start.8 = (bf16[128,256]{1,0:T(8,128)(2,1)S(1)}, bf16[128,256]{1,0:T(8,128)(2,1)}, u32[]{:S(2)}) copy-start(bf16[128,256]{1,0:T(8,128)(2,1)} %param.25) | copy-start | bytes 196612
  134.5 18.7 %copy-start.9 = (f32[128,256]{1,0:T(8,128)S(1)}, f32[128,256]{1,0:T(8,128)}, u32[]{:S(2)}) copy-start(f32[128,256]{1,0:T(8,128)} %get-tuple-element.24) | copy-start | bytes 393220
  136.1 1.0 copy-start.1

commit v2 on v1

--- a/solution.py
+++ b/solution.py
@@ -9,6 +9,11 @@
 
 MESH = pl.DeviceIdType.MESH
 VMEM_LIMIT = 56 * 1024 * 1024
+
+
+def sides(m):
+    high = max(d for d in range(1, m + 1) if m % d == 0 and d * d <= m)
+    return high, m // high
 
 
 def greet(n, m, me, j):
@@ -56,7 +61,7 @@
 
 def dispatch_kernel(
     n, m, xs, ys, keep, driven, xo, yo, hidden, prev, carry,
-    cum, loc, s1s, s1r, s2s, s2r, cs, cr, lsem,
+    cum, loc, s1s, s1r, f1s, f1r, f2s, f2r, cs, cr, lsem,
 ):
     me, j = lax.axis_index("sp"), lax.axis_index("tp")
     cap, q = xs.shape[0] // n, xs.shape[1]
@@ -64,6 +69,16 @@
     rows = lambda s: pl.ds(pl.multiple_of(s * cap, cap), cap)
     cols = lambda t: pl.ds(pl.multiple_of(t * q, q), q)
     pairs = ((0, xs, xo), (1, ys, yo))
+    high, low = sides(m)
+    upper, lower = lax.div(j, low), lax.rem(j, low)
+
+    def size(i):
+        return low if i == 0 else high
+
+    def near(i, along, across):
+        up, down = (across, along) if i == 0 else (along, across)
+        return lax.rem(upper + up, high) * low + lax.rem(lower + down, low)
+
     a, b = scan_rows(keep[...], driven[...], False)
     cum[...] = a
     loc[...] = b
@@ -104,25 +119,41 @@
 
     lax.fori_loop(1, n, start_first, 0)
 
-    def forward(source):
-        for p in range(1, m):
-            for i, _, o in pairs:
-                block = o.at[rows(source), cols(j)]
-                send(block, block, s2s.at[i, p], s2r.at[i, p], {"tp": lax.rem(j + p, m)}).start()
+    def onward(k, i, o):
+        source = lax.rem(me - k + n, n)
+        block = o.at[rows(source), cols(j)]
+        for p in range(1, size(i)):
+            send(block, block, f1s.at[i, p], f1r.at[i, p, k], {"tp": near(i, p, 0)}).start()
+        for p in range(1, size(1 - i)):
+            send(block, block, f2s.at[i, p, 0], f2r.at[i, p, 0], {"tp": near(i, 0, p)}).start()
+
+    def relayed(k, i, o):
+        source = lax.rem(me - k + n, n)
+        for c in range(1, size(i)):
+            far = near(i, size(i) - c, 0)
+            block = o.at[rows(source), cols(far)]
+            send(block, block, f1s.at[i, c], f1r.at[i, c, k], {"tp": far}).wait_recv()
+            for p in range(1, size(1 - i)):
+                send(block, block, f2s.at[i, p, c], f2r.at[i, p, c], {"tp": near(i, 0, p)}).start()
 
     for c in own:
         c.wait()
-    forward(me)
+    for i, _, o in pairs:
+        onward(0, i, o)
 
     def relay(k, _):
         source = lax.rem(me - k + n, n)
         for i, s, o in pairs:
             block = o.at[rows(source), cols(j)]
             send(block, block, s1s.at[i], s1r.at[i, k], {"sp": source}).wait_recv()
-        forward(source)
+            onward(k, i, o)
+        for i, s, o in pairs:
+            relayed(k - 1, i, o)
         return 0
 
     lax.fori_loop(1, n, relay, 0)
+    for i, _, o in pairs:
+        relayed(n - 1, i, o)
 
     def take_carry(k, _):
         source = lax.rem(me - k + n, n)
@@ -141,16 +172,22 @@
     for i, s, o in pairs:
         part = s.at[pl.ds(0, (n - 1) * cap)]
         send(part, part, s1s.at[i], s1r.at[i, 0], {"sp": lax.rem(me + 1, n)}).wait_send()
-        for p in range(1, m):
-            far = lax.rem(j - p + m, m)
-            mine, theirs = o.at[:, cols(j)], o.at[:, cols(far)]
-            send(mine, mine, s2s.at[i, p], s2r.at[i, p], {"tp": far}).wait_send()
-            send(theirs, theirs, s2s.at[i, p], s2r.at[i, p], {"tp": far}).wait_recv()
+        mine = o.at[:, cols(j)]
+        for p in range(1, size(i)):
+            send(mine, mine, f1s.at[i, p], f1r.at[i, p, 0], {"tp": near(i, p, 0)}).wait_send()
+        for p in range(1, size(1 - i)):
+            for c in range(size(i)):
+                sent = o.at[:, cols(near(i, size(i) - c, 0))]
+                came = o.at[:, cols(near(i, size(i) - c, size(1 - i) - p))]
+                to = {"tp": near(i, 0, p)}
+                send(sent, sent, f2s.at[i, p, c], f2r.at[i, p, c], to).wait_send()
+                send(came, came, f2s.at[i, p, c], f2r.at[i, p, c], to).wait_recv()
 
 
 def return_kernel(
-    n, m, pr, pick, hid, out, hid_all,
-    stage, red, back, rs, rr, bs, br, gs, gr, hs, hr, lsem,
+    n, m, pr, pick, hid, cot, nrm, gain, irms, omat, keep, carry, total_out, gow,
+    out, hid_all, stage, red, back, mix_t, got, cum, loc, enters,
+    rs, rr, bs, br, gs, gr, hs, hr, ms, mr, cs, cr, lsem,
 ):
     me, j = lax.axis_index("sp"), lax.axis_index("tp")
     tok = hid.shape[0]
@@ -236,35 +273,40 @@
         send(mine, mine, gs.at[p], gr.at[p], {"tp": far}).wait_send()
         send(theirs, theirs, gs.at[p], gr.at[p], {"tp": far}).wait_recv()
 
-
-def last_kernel(
-    n, m, mix_t, hid_all, d_state, keep, carry, total, gow,
-    got, cum, loc, back, ms, mr, cs, cr, lsem,
-):
-    me, j = lax.axis_index("sp"), lax.axis_index("tp")
-    tok, width = keep.shape
     slab = mix_t.shape[0] // n
-    rows = lambda s: pl.ds(pl.multiple_of(s * slab, slab), slab)
-    greet(n, m, me, j)
-    own = pltpu.make_async_copy(mix_t.at[rows(me)], got.at[me], lsem)
-    own.start()
+    width = keep.shape[1]
+    slabs = lambda s: pl.ds(pl.multiple_of(s * slab, slab), slab)
+    scale = gain[...]
+    nhat = nrm[...].astype(jnp.float32) / scale
+    gained = scale * out[...].astype(jnp.float32)
+    stat = jnp.mean(gained * nhat, axis=1, keepdims=True)
+    mixed = cot[...].astype(jnp.float32) + irms[...] * (gained - nhat * stat)
+    mix_t[...] = mixed.T.astype(mix_t.dtype)
+    loc[...] = jnp.dot(
+        mixed.astype(omat.dtype), omat[...], preferred_element_type=jnp.float32
+    )
 
     def blocks(k):
         to = lax.rem(me + k, n)
-        return send(mix_t.at[rows(to)], got.at[me], ms.at[k], mr.at[k], {"sp": to})
+        return send(mix_t.at[slabs(to)], got.at[me], ms.at[k], mr.at[k], {"sp": to})
 
     def carried(k):
         to = lax.rem(me + k, n)
-        return send(back.at[me], back.at[me], cs.at[k], cr.at[k], {"sp": to})
-
+        return send(enters.at[me], enters.at[me], cs.at[k], cr.at[k], {"sp": to})
+
+    def start_blocks(k, _):
+        blocks(k).start()
+        return 0
+
+    lax.fori_loop(1, n, start_blocks, 0)
     place = lax.broadcasted_iota(jnp.int32, (tok, width), 0)
     here = keep[...]
     after = jnp.where(place < tok - 1, pltpu.roll(here, tok - 1, 0), 1.0)
-    a, b = scan_rows(after, d_state[...], True)
+    a, b = scan_rows(after, loc[...], True)
+    enters[me] = jnp.broadcast_to(here[0:1] * b[0:1], (8, width))
     cum[...] = a
     loc[...] = b
-    back[me] = jnp.broadcast_to(here[0:1] * b[0:1], (8, width))
-    own.wait()
+    gow[...] = jnp.dot(mix_t[slabs(me)], hid_all[me], preferred_element_type=jnp.float32)
 
     def start(k, _):
         carried(k).start()
@@ -272,33 +314,26 @@
 
     lax.fori_loop(1, n, start, 0)
 
-    def start_blocks(k, _):
-        blocks(k).start()
-        return 0
-
-    lax.fori_loop(1, n, start_blocks, 0)
+    def add(k, _):
+        source = lax.rem(me - k + n, n)
+        send(got.at[source], got.at[source], ms.at[k], mr.at[k], {"sp": source}).wait_recv()
+        blocks(k).wait_send()
+        gow[...] += jnp.dot(got[source], hid_all[source], preferred_element_type=jnp.float32)
+        return 0
+
+    lax.fori_loop(1, n, add, 0)
 
     def take(k, _):
         source = lax.rem(me - k + n, n)
-        send(back.at[source], back.at[source], cs.at[k], cr.at[k], {"sp": source}).wait_recv()
+        send(enters.at[source], enters.at[source], cs.at[k], cr.at[k], {"sp": source}).wait_recv()
         carried(k).wait_send()
         return 0
 
     lax.fori_loop(1, n, take, 0)
     enter = jnp.zeros((1, width), jnp.float32)
     for s in range(n - 1, -1, -1):
-        enter = jnp.where(s > me, carry[s, 0:1] * enter + back[s, 0:1], enter)
-    total[...] = loc[...] + cum[...] * enter
-    gow[...] = jnp.dot(got[me], hid_all[me], preferred_element_type=jnp.float32)
-
-    def add(k, _):
-        source = lax.rem(me - k + n, n)
-        send(got.at[source], got.at[source], ms.at[k], mr.at[k], {"sp": source}).wait_recv()
-        blocks(k).wait_send()
-        gow[...] += jnp.dot(got[source], hid_all[source], preferred_element_type=jnp.float32)
-        return 0
-
-    lax.fori_loop(1, n, add, 0)
+        enter = jnp.where(s > me, carry[s, 0:1] * enter + enters[s, 0:1], enter)
+    total_out[...] = loc[...] + cum[...] * enter
 
 
 def call(kernel, n, m, outs, scratch, ident, *args):
@@ -337,6 +372,7 @@
     capacity = 2 * picks * tok_rows // n
     slots = n * capacity
     q = features // m
+    wide = max(sides(m))
     channels = recurrence_input.shape[1]
     f32, bf16 = jnp.float32, jnp.bfloat16
     dma = pltpu.SemaphoreType.DMA
@@ -391,8 +427,10 @@
             pltpu.VMEM((tok_rows, channels), f32),
             dma((2,)),
             dma((2, n)),
-            dma((2, m)),
-            dma((2, m)),
+            dma((2, wide)),
+            dma((2, wide, n)),
+            dma((2, wide, wide)),
+            dma((2, wide, wide)),
             dma((n,)),
             dma((n,)),
             dma((2,)),
@@ -417,49 +455,45 @@
     partial_rows = lax.dot_general(d_gate, gate_w, coldims, preferred_element_type=f32)
     partial_rows = partial_rows + lax.dot_general(d_up, up_w, coldims, preferred_element_type=f32)
 
-    d_norm, hidden_all = call(
+    total, grad_out_weight = call(
         return_kernel, n, m,
-        [((tok_rows, features), bf16), ((n, tok_rows, channels), bf16)],
+        [((tok_rows, channels), f32), ((features // n, channels), f32)],
         [
+            pltpu.VMEM((tok_rows, features), bf16),
+            pltpu.VMEM((n, tok_rows, channels), bf16),
             pltpu.VMEM((m - 1, slots, q), bf16),
             pltpu.VMEM((slots, q), bf16),
             pltpu.VMEM((slots, q), bf16),
-            dma((n + 1,)),
-            dma((n + 1,)),
-            dma((n,)),
-            dma((n,)),
-            dma((m,)),
-            dma((m,)),
-            dma((n,)),
-            dma((n,)),
-            dma,
-        ],
-        1, partial_rows.astype(bf16), pick, hidden,
-    )
-    d_norm = d_norm.astype(f32)
-    nhat = normed.astype(f32) / expert_norm_scale[None, :]
-    gained = expert_norm_scale[None, :] * d_norm
-    stat = jnp.mean(gained * nhat, axis=1, keepdims=True)
-    d_mix = (
-        cotangent.astype(f32) + inverse_root_mean_square[:, None] * (gained - nhat * stat)
-    ).astype(bf16)
-    d_state = jnp.dot(d_mix, output_matrix, preferred_element_type=f32)
-
-    total, grad_out_weight = call(
-        last_kernel, n, m,
-        [((tok_rows, channels), f32), ((features // n, channels), f32)],
-        [
+            pltpu.VMEM((features, tok_rows), bf16),
             pltpu.VMEM((n, features // n, tok_rows), bf16),
             pltpu.VMEM((tok_rows, channels), f32),
             pltpu.VMEM((tok_rows, channels), f32),
             pltpu.VMEM((n, 8, channels), f32),
+            dma((n + 1,)),
+            dma((n + 1,)),
+            dma((n,)),
+            dma((n,)),
+            dma((m,)),
+            dma((m,)),
+            dma((n,)),
+            dma((n,)),
             dma((n,)),
             dma((n,)),
             dma((n,)),
             dma((n,)),
             dma,
         ],
-        2, d_mix.T, hidden_all, d_state, keep, carry,
+        1,
+        partial_rows.astype(bf16),
+        pick,
+        hidden,
+        cotangent,
+        normed,
+        expert_norm_scale[None, :],
+        inverse_root_mean_square[:, None],
+        output_matrix,
+        keep,
+        carry,
     )
     grad_rec_input = total * scale_in * admit
     grad_input_gate = total * scale_in * signal * admit * (1.0 - admit)

time: 158 us -> 146 us (0.924)
  Pallas kernels: 116 us -> 111 us
  local copies, waits for them, and re-layouts: 8.37 us -> 5.43 us
  other arithmetic: 8 us -> 6.11 us
    pallas_call x3 -> x2, Pallas kernels: 116 us -> 111 us  [call(): pl.pallas_call(functools.partial(kernel, n, m), out_shape=tuple((jax.Shap...]
    unnamed x34 -> x24, local copies, waits for them, and re-layouts: 5.96 us -> 3.6 us
where the time goes in v2:
time: 146 us
  Pallas kernels  111 us (76%)
  matrix products  22 us (15%)
  other arithmetic  6.11 us (4%)
  local copies, waits for them, and re-layouts  5.43 us (4%)
    pallas_call x2, Pallas kernels, call(): pl.pallas_call(functools.partial(kernel, n, m), out_shape=tuple((jax.Shap...  111 us
    unnamed x24, local copies, waits for them, and re-layouts  3.6 us
    dot_general x1, matrix products, shards(): gate_pre = jnp.dot(token_recv, gate_w, preferred_element_type=f32)  2.98 us

profile of v2, /device:TPU:0, one launch (start us, length us, event | category | flops | bytes accessed | tf_op | source)
XLA Modules:
  0.0 145.6 jit_solution(17556477380898255718)
XLA Ops:
  0.6 0.0 copy-start
  0.7 0.9 copy.35
  1.6 0.1 eq.72
  1.7 0.2 fusion.13
  1.9 0.1 convert_element_type.50
  2.1 0.1 copy.36
  2.1 0.7 multiply_add_fusion.1
  2.9 2.0 %convolution_convert_fusion.3.xs = bf16[512,512]{1,0:T(8,128)(2,1)} fusion(bf16[128,2048]{1,0:T(8,128)(2,1)} %nrm.1, s32[]{:T(128)S(6)} %select_n.20, s32[128]{0:T(128)S(1)} %get-tuple-element.31, s32[128]{0:T(128)S(1)} %get-tuple-element.30), kind=kOutput, calls=%fused_computation.18 | convolution fusion | flops 67567616 | bytes 656388 | tf_op jit(solution)/shard_map/dot_general | solution.py:402
  4.9 0.8 slice_bitcast_fusion
  5.6 0.2 select_reduce_fusion
  5.8 2.0 %fusion.12.ys = bf16[512,512]{1,0:T(8,128)(2,1)} fusion(f32[512]{0:T(512)S(1)} %add.39, bf16[128,2048]{1,0:T(8,128)(2,1)} %cot.1, s32[]{:T(128)S(6)} %select_n.20, s32[128]{0:T(128)S(1)} %get-tuple-element.31, s32[128]{0:T(128)S(1)} %get-tuple-element.30), kind=kOutput, calls=%fused_computation.17 | convolution fusion | flops 67829760 | bytes 658436 | tf_op jit(solution)/shard_map/dot_general | solution.py:404
  7.8 0.7 fusion.37
  8.5 1.8 %convert_multiply_fusion.2 = (f32[128,256]{1,0:T(8,128)}, f32[128,256]{1,0:T(8,128)}) fusion(bf16[128,256]{1,0:T(8,128)(2,1)} %param.24, bf16[128,256]{1,0:T(8,128)(2,1)} %param.26, f32[128,256]{1,0:T(8,128)} %param.28, f32[256]{0:T(256)S(1)} %fusion.37, bf16[128,256]{1,0:T(8,128)(2,1)} %param.25), kind=kLoop, calls=%fused_computation.39 | loop fusion | flops 491520 | bytes 590848 | tf_op jit(solution)/shard_map/mul | solution.py:414
  10.4 50.6 %shard_map.198 = (bf16[512,2048]{1,0:T(8,128)(2,1)}, bf16[512,2048]{1,0:T(8,128)(2,1)}, bf16[128,256]{1,0:T(8,128)(2,1)}, f32[128,256]{1,0:T(8,128)}, f32[8,8,256]{2,1,0:T(8,128)}) custom-call(bf16[512,512]{1,0:T(8,128)(2,1)} %convolution_convert_fusion.3.xs, bf16[512,512]{1,0:T(8,128)(2,1)} %fusion.12.ys, f32[128,256]{1,0:T(8,128)} %get-tuple-element.27.keep, ...), custom_call_target="tpu_custom_call" | custom-call | tf_op jit(solution)/shard_map/pallas_call | solution.py:340
  60.9 0.0 copy-done
  60.9 0.0 copy-start.1
  61.0 0.0 copy-start.10
  61.0 3.0 %fusion.5 = f32[512,512]{1,0:T(8,128)S(1)} fusion(bf16[512,2048]{1,0:T(8,128)(2,1)} %get-tuple-element.14, bf16[1,2048,512]{2,1,0:T(8,128)(2,1)S(1)} %copy-done), kind=kOutput, calls=%fused_computation.9 | convolution fusion | flops 1073741824 | bytes 5242880 | tf_op jit(solution)/shard_map/dot_general | solution.py:444
  64.0 0.0 copy-done.1
  64.0 0.0 copy-done.10
  64.0 0.0 copy-start.8
  64.0 0.0 copy-start.9
  64.0 1.3 fusion.8
  65.3 0.3 copy-done.8
  65.6 0.6 copy-done.9
  66.2 1.6 %multiply_convert_fusion.1 = (bf16[512,512]{1,0:T(8,128)(2,1)S(1)}, bf16[512,512]{1,0:T(8,128)(2,1)S(1)}) fusion(f32[512,512]{1,0:T(8,128)S(1)} %fusion.5, f32[512,512]{1,0:T(8,128)S(1)} %fusion.8, bf16[512,2048]{1,0:T(8,128)(2,1)S(1)} %copy-done.9, bf16[1,512,2048]{2,1,0:T(8,128)(2,1)S(1)} %copy-done.8), kind=kOutput, calls=%fused_computation.22 | convolution fusion | flops 1077149696 | bytes 7340032 | tf_op jit(solution)/shard_map/dot_general | solution.py:449
  67.8 2.6 %fusion = bf16[1,2048,512]{2,1,0:T(8,128)(2,1)} fusion(bf16[512,2048]{1,0:T(8,128)(2,1)S(1)} %copy-done.10, bf16[512,512]{1,0:T(8,128)(2,1)S(1)} %get-tuple-element.22), kind=kOutput, calls=%fused_computation.4 | convolution fusion | flops 1074790400 | bytes 4718592 | tf_op jit(solution)/shard_map/dot_general | solution.py:453
  70.4 2.6 %fusion.1 = bf16[1,2048,512]{2,1,0:T(8,128)(2,1)} fusion(bf16[512,2048]{1,0:T(8,128)(2,1)S(1)} %copy-done.10, bf16[512,512]{1,0:T(8,128)(2,1)S(1)} %get-tuple-element.21), kind=kOutput, calls=%fused_computation.5 | convolution fusion | flops 1074790400 | bytes 4718592 | tf_op jit(solution)/shard_map/dot_general | solution.py:454
  73.1 2.7 %fusion.2 = bf16[1,512,2048]{2,1,0:T(8,128)(2,1)} fusion(bf16[512,2048]{1,0:T(8,128)(2,1)S(1)} %copy-done.9, f32[512,512]{1,0:T(8,128)S(1)} %fusion.8, f32[512,512]{1,0:T(8,128)S(1)} %fusion.5), kind=kOutput, calls=%fused_computation.6 | convolution fusion | flops 1076363264 | bytes 6291456 | tf_op jit(solution)/shard_map/dot_general | solution.py:452
  75.8 1.3 fusion.3
  77.1 0.0 copy-start.7
  77.1 2.6 %add_convert_fusion.pr = bf16[512,2048]{1,0:T(8,128)(2,1)} fusion(f32[512,2048]{1,0:T(8,128)S(1)} %fusion.3, bf16[512,512]{1,0:T(8,128)(2,1)S(1)} %get-tuple-element.21, bf16[1,2048,512]{2,1,0:T(8,128)(2,1)S(1)} %copy-done.1), kind=kOutput, calls=%fused_computation | convolution fusion | flops 1075838976 | bytes 8912896 | tf_op jit(solution)/shard_map/dot_general | solution.py:456
  79.8 0.8 fusion.17.pick
  80.5 0.0 copy-done.7
  80.5 0.7 copy.37.irms
  81.3 0.0 copy-start.2
  81.3 0.0 copy-start.3
  81.3 0.0 copy-start.4
  81.3 0.0 copy-start.5
  81.3 0.0 copy-start.6
  81.3 60.8 %shard_map.199 = (f32[128,256]{1,0:T(8,128)}, f32[256,256]{1,0:T(8,128)}) custom-call(bf16[512,2048]{1,0:T(8,128)(2,1)} %add_convert_fusion.pr, bf16[128,512]{1,0:T(8,128)(2,1)} %fusion.17.pick, bf16[128,256]{1,0:T(8,128)(2,1)} %get-tuple-element.16.hid, bf16[128,2048]{1,0:T(8,128)(2,1)} %cot.1, bf16[128,2048]{1,0:T(8,128)(2,1)} %nrm.1, f32[1,2048]{1,0:T(1,128)} %bitcast.41, ...), custom_call_target="tpu_custom_call" | custom-call | tf_op jit(solution)/shard_map/pallas_call | solution.py:340
  142.1 0.0 copy-done.2
  142.1 0.0 copy-done.3
  142.1 0.0 copy-done.4
  142.1 0.0 copy-done.5
  142.1 0.0 copy-done.6
  142.1 1.9 %fusion.22 = (f32[128,256]{1,0:T(8,128)}, f32[128,256]{1,0:T(8,128)}, f32[128,256]{1,0:T(8,128)}) fusion(bf16[128,256]{1,0:T(8,128)(2,1)S(1)} %copy-done.3, f32[128,256]{1,0:T(8,128)} %get-tuple-element.19, bf16[128,256]{1,0:T(8,128)(2,1)S(1)} %copy-done.4, f32[128,256]{1,0:T(8,128)S(1)} %copy-done.2, f32[256]{0:T(256)S(1)} %fusion.37, ...), kind=kLoop, calls=%fused_computation.41 | loop fusion | flops 1015808 | bytes 984064 | tf_op jit(solution)/shard_map/mul | solution.py:499
  144.0 1.7 %copy.39 = f32[256,256]{1,0:T(8,128)} copy(f32[256,256]{1,0:T(8,128)} %get-tuple-element.44) | data formatting | bytes 524288
  (3 shorter events, 0.0 us)
Async XLA Ops:
  0.6 60.3 %copy-start = (bf16[1,2048,512]{2,1,0:T(8,128)(2,1)S(1)}, bf16[1,2048,512]{2,1,0:T(8,128)(2,1)}, u32[]{:S(2)}) copy-start(bf16[1,2048,512]{2,1,0:T(8,128)(2,1)} %param.21) | copy-start | bytes 6291460
  60.9 3.0 %copy-start.1 = (bf16[1,2048,512]{2,1,0:T(8,128)(2,1)S(1)}, bf16[1,2048,512]{2,1,0:T(8,128)(2,1)}, u32[]{:S(2)}) copy-start(bf16[1,2048,512]{2,1,0:T(8,128)(2,1)} %param.22) | copy-start | bytes 6291460
  61.0 3.0 %copy-start.10 = (bf16[512,2048]{1,0:T(8,128)(2,1)S(1)}, bf16[512,2048]{1,0:T(8,128)(2,1)}, u32[]{:S(2)}) copy-start(bf16[512,2048]{1,0:T(8,128)(2,1)} %get-tuple-element.14) | copy-start | bytes 6291460
  64.0 1.6 %copy-start.8 = (bf16[1,512,2048]{2,1,0:T(8,128)(2,1)S(1)}, bf16[1,512,2048]{2,1,0:T(8,128)(2,1)}, u32[]{:S(2)}) copy-start(bf16[1,512,2048]{2,1,0:T(8,128)(2,1)} %param.23) | copy-start | bytes 6291460
  64.0 2.2 %copy-start.9 = (bf16[512,2048]{1,0:T(8,128)(2,1)S(1)}, bf16[512,2048]{1,0:T(8,128)(2,1)}, u32[]{:S(2)}) copy-start(bf16[512,2048]{1,0:T(8,128)(2,1)} %get-tuple-element.15) | copy-start | bytes 6291460
  77.1 3.4 %copy-start.7 = (f32[128]{0:T(128)S(1)}, f32[128]{0:T(128)}, u32[]{:S(2)}) copy-start(f32[128]{0:T(128)} %param.17) | copy-start | bytes 1540
  81.3 60.8 %copy-start.2 = (f32[128,256]{1,0:T(8,128)S(1)}, f32[128,256]{1,0:T(8,128)}, u32[]{:S(2)}) copy-start(f32[128,256]{1,0:T(8,128)} %param.28) | copy-start | bytes 393220
  81.3 60.8 %copy-start.3 = (bf16[128,256]{1,0:T(8,128)(2,1)S(1)}, bf16[128,256]{1,0:T(8,128)(2,1)}, u32[]{:S(2)}) copy-start(bf16[128,256]{1,0:T(8,128)(2,1)} %param.24) | copy-start | bytes 196612
  81.3 60.8 %copy-start.4 = (bf16[128,256]{1,0:T(8,128)(2,1)S(1)}, bf16[128,256]{1,0:T(8,128)(2,1)}, u32[]{:S(2)}) copy-start(bf16[128,256]{1,0:T(8,128)(2,1)} %param.26) | copy-start | bytes 196612
  81.3 60.8 %copy-start.5 = (bf16[128,256]{1,0:T(8,128)(2,1)S(1)}, bf16[128,256]{1,0:T(8,128)(2,1)}, u32[]{:S(2)}) copy-start(bf16[128,256]{1,0:T(8,128)(2,1)} %param.25) | copy-start | bytes 196612
  81.3 60.8 %copy-start.6 = (f32[128,256]{1,0:T(8,128)S(1)}, f32[128,256]{1,0:T(8,128)}, u32[]{:S(2)}) copy-start(f32[128,256]{1,0:T(8,128)} %get-tuple-element.20) | copy-start | bytes 393220

commit v3 on v2

--- a/solution.py
+++ b/solution.py
@@ -336,12 +336,15 @@
     total_out[...] = loc[...] + cum[...] * enter
 
 
-def call(kernel, n, m, outs, scratch, ident, *args):
+def call(kernel, n, m, outs, scratch, ident, *args, loose=0):
     return pl.pallas_call(
         functools.partial(kernel, n, m),
         out_shape=tuple(jax.ShapeDtypeStruct(s, d) for s, d in outs),
         in_specs=[pl.BlockSpec(memory_space=pltpu.VMEM)] * len(args),
-        out_specs=tuple(pl.BlockSpec(memory_space=pltpu.VMEM) for _ in outs),
+        out_specs=tuple(
+            pl.BlockSpec(memory_space=pl.ANY if at < loose else pltpu.VMEM)
+            for at in range(len(outs))
+        ),
         scratch_shapes=scratch,
         compiler_params=pltpu.CompilerParams(
             collective_id=ident, has_side_effects=True, vmem_limit_bytes=VMEM_LIMIT
@@ -435,7 +438,7 @@
             dma((n,)),
             dma((2,)),
         ],
-        0, token_send, grad_send, keep, driven,
+        0, token_send, grad_send, keep, driven, loose=2,
     )
 
     gate_w = gate_weight[0]

time: 146 us -> 145 us (level)
  no operation moved by 1% of the time
where the time goes in v3:
time: 145 us
  Pallas kernels  111 us (77%)
  matrix products  22 us (15%)
  other arithmetic  6.11 us (4%)
  local copies, waits for them, and re-layouts  5.43 us (4%)
    pallas_call x2, Pallas kernels, call(): pl.pallas_call(functools.partial(kernel, n, m), out_shape=tuple((jax.Shap...  111 us
    unnamed x24, local copies, waits for them, and re-layouts  3.59 us
    dot_general x1, matrix products, shards(): gate_pre = jnp.dot(token_recv, gate_w, preferred_element_type=f32)  2.99 us

profile of v3, /device:TPU:0, one launch (start us, length us, event | category | flops | bytes accessed | tf_op | source)
XLA Modules:
  0.0 145.0 jit_solution(3715386336018353279)
XLA Ops:
  0.6 0.0 copy-start
  0.7 0.9 copy.35
  1.6 0.1 eq.72
  1.7 0.2 fusion.13
  1.9 0.1 convert_element_type.50
  2.1 0.1 copy.36
  2.1 0.7 multiply_add_fusion.1
  2.9 2.0 %convolution_convert_fusion.3.xs = bf16[512,512]{1,0:T(8,128)(2,1)} fusion(bf16[128,2048]{1,0:T(8,128)(2,1)} %nrm.1, s32[]{:T(128)S(6)} %select_n.20, s32[128]{0:T(128)S(1)} %get-tuple-element.31, s32[128]{0:T(128)S(1)} %get-tuple-element.30), kind=kOutput, calls=%fused_computation.18 | convolution fusion | flops 67567616 | bytes 656388 | tf_op jit(solution)/shard_map/dot_general | solution.py:405
  4.9 0.8 slice_bitcast_fusion
  5.6 0.2 select_reduce_fusion
  5.8 2.0 %fusion.12.ys = bf16[512,512]{1,0:T(8,128)(2,1)} fusion(f32[512]{0:T(512)S(1)} %add.39, bf16[128,2048]{1,0:T(8,128)(2,1)} %cot.1, s32[]{:T(128)S(6)} %select_n.20, s32[128]{0:T(128)S(1)} %get-tuple-element.31, s32[128]{0:T(128)S(1)} %get-tuple-element.30), kind=kOutput, calls=%fused_computation.17 | convolution fusion | flops 67829760 | bytes 658436 | tf_op jit(solution)/shard_map/dot_general | solution.py:407
  7.8 0.7 fusion.37
  8.5 1.8 %convert_multiply_fusion.2 = (f32[128,256]{1,0:T(8,128)}, f32[128,256]{1,0:T(8,128)}) fusion(bf16[128,256]{1,0:T(8,128)(2,1)} %param.24, bf16[128,256]{1,0:T(8,128)(2,1)} %param.26, f32[128,256]{1,0:T(8,128)} %param.28, f32[256]{0:T(256)S(1)} %fusion.37, bf16[128,256]{1,0:T(8,128)(2,1)} %param.25), kind=kLoop, calls=%fused_computation.39 | loop fusion | flops 491520 | bytes 590848 | tf_op jit(solution)/shard_map/mul | solution.py:417
  10.4 49.9 %shard_map.198 = (bf16[512,2048]{1,0:T(8,128)(2,1)}, bf16[512,2048]{1,0:T(8,128)(2,1)}, bf16[128,256]{1,0:T(8,128)(2,1)}, f32[128,256]{1,0:T(8,128)}, f32[8,8,256]{2,1,0:T(8,128)}) custom-call(bf16[512,512]{1,0:T(8,128)(2,1)} %convolution_convert_fusion.3.xs, bf16[512,512]{1,0:T(8,128)(2,1)} %fusion.12.ys, f32[128,256]{1,0:T(8,128)} %get-tuple-element.27.keep, ...), custom_call_target="tpu_custom_call" | custom-call | tf_op jit(solution)/shard_map/pallas_call | solution.py:340
  60.3 0.0 copy-done
  60.3 0.0 copy-start.1
  60.3 0.0 copy-start.10
  60.3 3.0 %fusion.5 = f32[512,512]{1,0:T(8,128)S(1)} fusion(bf16[512,2048]{1,0:T(8,128)(2,1)} %get-tuple-element.14, bf16[1,2048,512]{2,1,0:T(8,128)(2,1)S(1)} %copy-done), kind=kOutput, calls=%fused_computation.9 | convolution fusion | flops 1073741824 | bytes 5242880 | tf_op jit(solution)/shard_map/dot_general | solution.py:447
  63.3 0.0 copy-done.1
  63.3 0.0 copy-done.10
  63.3 0.0 copy-start.8
  63.3 0.0 copy-start.9
  63.3 1.3 fusion.8
  64.6 0.3 copy-done.8
  64.9 0.6 copy-done.9
  65.5 1.6 %multiply_convert_fusion.1 = (bf16[512,512]{1,0:T(8,128)(2,1)S(1)}, bf16[512,512]{1,0:T(8,128)(2,1)S(1)}) fusion(f32[512,512]{1,0:T(8,128)S(1)} %fusion.5, f32[512,512]{1,0:T(8,128)S(1)} %fusion.8, bf16[512,2048]{1,0:T(8,128)(2,1)S(1)} %copy-done.9, bf16[1,512,2048]{2,1,0:T(8,128)(2,1)S(1)} %copy-done.8), kind=kOutput, calls=%fused_computation.22 | convolution fusion | flops 1077149696 | bytes 7340032 | tf_op jit(solution)/shard_map/dot_general | solution.py:452
  67.1 2.6 %fusion = bf16[1,2048,512]{2,1,0:T(8,128)(2,1)} fusion(bf16[512,2048]{1,0:T(8,128)(2,1)S(1)} %copy-done.10, bf16[512,512]{1,0:T(8,128)(2,1)S(1)} %get-tuple-element.22), kind=kOutput, calls=%fused_computation.4 | convolution fusion | flops 1074790400 | bytes 4718592 | tf_op jit(solution)/shard_map/dot_general | solution.py:456
  69.8 2.6 %fusion.1 = bf16[1,2048,512]{2,1,0:T(8,128)(2,1)} fusion(bf16[512,2048]{1,0:T(8,128)(2,1)S(1)} %copy-done.10, bf16[512,512]{1,0:T(8,128)(2,1)S(1)} %get-tuple-element.21), kind=kOutput, calls=%fused_computation.5 | convolution fusion | flops 1074790400 | bytes 4718592 | tf_op jit(solution)/shard_map/dot_general | solution.py:457
  72.4 2.7 %fusion.2 = bf16[1,512,2048]{2,1,0:T(8,128)(2,1)} fusion(bf16[512,2048]{1,0:T(8,128)(2,1)S(1)} %copy-done.9, f32[512,512]{1,0:T(8,128)S(1)} %fusion.8, f32[512,512]{1,0:T(8,128)S(1)} %fusion.5), kind=kOutput, calls=%fused_computation.6 | convolution fusion | flops 1076363264 | bytes 6291456 | tf_op jit(solution)/shard_map/dot_general | solution.py:455
  75.1 1.3 fusion.3
  76.5 0.0 copy-start.7
  76.5 2.6 %add_convert_fusion.pr = bf16[512,2048]{1,0:T(8,128)(2,1)} fusion(f32[512,2048]{1,0:T(8,128)S(1)} %fusion.3, bf16[512,512]{1,0:T(8,128)(2,1)S(1)} %get-tuple-element.21, bf16[1,2048,512]{2,1,0:T(8,128)(2,1)S(1)} %copy-done.1), kind=kOutput, calls=%fused_computation | convolution fusion | flops 1075838976 | bytes 8912896 | tf_op jit(solution)/shard_map/dot_general | solution.py:459
  79.1 0.8 fusion.17.pick
  79.8 0.0 copy-done.7
  79.8 0.7 copy.37.irms
  80.6 0.0 copy-start.2
  80.6 0.0 copy-start.3
  80.6 0.0 copy-start.4
  80.6 0.0 copy-start.5
  80.6 0.0 copy-start.6
  80.6 60.8 %shard_map.199 = (f32[128,256]{1,0:T(8,128)}, f32[256,256]{1,0:T(8,128)}) custom-call(bf16[512,2048]{1,0:T(8,128)(2,1)} %add_convert_fusion.pr, bf16[128,512]{1,0:T(8,128)(2,1)} %fusion.17.pick, bf16[128,256]{1,0:T(8,128)(2,1)} %get-tuple-element.16.hid, bf16[128,2048]{1,0:T(8,128)(2,1)} %cot.1, bf16[128,2048]{1,0:T(8,128)(2,1)} %nrm.1, f32[1,2048]{1,0:T(1,128)} %bitcast.41, ...), custom_call_target="tpu_custom_call" | custom-call | tf_op jit(solution)/shard_map/pallas_call | solution.py:340
  141.4 0.0 copy-done.2
  141.4 0.0 copy-done.3
  141.4 0.0 copy-done.4
  141.5 0.0 copy-done.5
  141.5 0.0 copy-done.6
  141.5 1.9 %fusion.22 = (f32[128,256]{1,0:T(8,128)}, f32[128,256]{1,0:T(8,128)}, f32[128,256]{1,0:T(8,128)}) fusion(bf16[128,256]{1,0:T(8,128)(2,1)S(1)} %copy-done.3, f32[128,256]{1,0:T(8,128)} %get-tuple-element.19, bf16[128,256]{1,0:T(8,128)(2,1)S(1)} %copy-done.4, f32[128,256]{1,0:T(8,128)S(1)} %copy-done.2, f32[256]{0:T(256)S(1)} %fusion.37, ...), kind=kLoop, calls=%fused_computation.41 | loop fusion | flops 1015808 | bytes 984064 | tf_op jit(solution)/shard_map/mul | solution.py:502
  143.4 1.7 %copy.39 = f32[256,256]{1,0:T(8,128)} copy(f32[256,256]{1,0:T(8,128)} %get-tuple-element.44) | data formatting | bytes 524288
  (3 shorter events, 0.0 us)
Async XLA Ops:
  0.6 59.6 %copy-start = (bf16[1,2048,512]{2,1,0:T(8,128)(2,1)S(1)}, bf16[1,2048,512]{2,1,0:T(8,128)(2,1)}, u32[]{:S(2)}) copy-start(bf16[1,2048,512]{2,1,0:T(8,128)(2,1)} %param.21) | copy-start | bytes 6291460
  60.3 3.0 %copy-start.1 = (bf16[1,2048,512]{2,1,0:T(8,128)(2,1)S(1)}, bf16[1,2048,512]{2,1,0:T(8,128)(2,1)}, u32[]{:S(2)}) copy-start(bf16[1,2048,512]{2,1,0:T(8,128)(2,1)} %param.22) | copy-start | bytes 6291460
  60.3 3.0 %copy-start.10 = (bf16[512,2048]{1,0:T(8,128)(2,1)S(1)}, bf16[512,2048]{1,0:T(8,128)(2,1)}, u32[]{:S(2)}) copy-start(bf16[512,2048]{1,0:T(8,128)(2,1)} %get-tuple-element.14) | copy-start | bytes 6291460
  63.3 1.6 %copy-start.8 = (bf16[1,512,2048]{2,1,0:T(8,128)(2,1)S(1)}, bf16[1,512,2048]{2,1,0:T(8,128)(2,1)}, u32[]{:S(2)}) copy-start(bf16[1,512,2048]{2,1,0:T(8,128)(2,1)} %param.23) | copy-start | bytes 6291460
  63.3 2.2 %copy-start.9 = (bf16[512,2048]{1,0:T(8,128)(2,1)S(1)}, bf16[512,2048]{1,0:T(8,128)(2,1)}, u32[]{:S(2)}) copy-start(bf16[512,2048]{1,0:T(8,128)(2,1)} %get-tuple-element.15) | copy-start | bytes 6291460
  76.5 3.4 %copy-start.7 = (f32[128]{0:T(128)S(1)}, f32[128]{0:T(128)}, u32[]{:S(2)}) copy-start(f32[128]{0:T(128)} %param.17) | copy-start | bytes 1540
  80.6 60.8 %copy-start.2 = (f32[128,256]{1,0:T(8,128)S(1)}, f32[128,256]{1,0:T(8,128)}, u32[]{:S(2)}) copy-start(f32[128,256]{1,0:T(8,128)} %param.28) | copy-start | bytes 393220
  80.6 60.8 %copy-start.3 = (bf16[128,256]{1,0:T(8,128)(2,1)S(1)}, bf16[128,256]{1,0:T(8,128)(2,1)}, u32[]{:S(2)}) copy-start(bf16[128,256]{1,0:T(8,128)(2,1)} %param.24) | copy-start | bytes 196612
  80.6 60.9 %copy-start.4 = (bf16[128,256]{1,0:T(8,128)(2,1)S(1)}, bf16[128,256]{1,0:T(8,128)(2,1)}, u32[]{:S(2)}) copy-start(bf16[128,256]{1,0:T(8,128)(2,1)} %param.26) | copy-start | bytes 196612
  80.6 60.9 %copy-start.5 = (bf16[128,256]{1,0:T(8,128)(2,1)S(1)}, bf16[128,256]{1,0:T(8,128)(2,1)}, u32[]{:S(2)}) copy-start(bf16[128,256]{1,0:T(8,128)(2,1)} %param.25) | copy-start | bytes 196612
  80.6 60.9 %copy-start.6 = (f32[128,256]{1,0:T(8,128)S(1)}, f32[128,256]{1,0:T(8,128)}, u32[]{:S(2)}) copy-start(f32[128,256]{1,0:T(8,128)} %get-tuple-element.20) | copy-start | bytes 393220
